TPU v7x, 32 devices: a whole 2x2x4 slice. The times are simulated.
32 devices in a mesh: sp: 16 (over z, y, x), tp: 2 (over core).
Axes of the slice: x: 2, y: 2, z: 4, core: 2. Of those that a mesh axis runs over, the one named last changes fastest.
Arguments:
- tokens: bfloat16 [8192, 3072], P('sp'), may hold values from -72 to 72
- w_query: bfloat16 [3072, 1024], P('sp', 'tp'), may hold values from -0.109375 to 0.109375
- w_key: bfloat16 [3072, 1024], P('sp', 'tp'), may hold values from -0.109375 to 0.109375
- w_value: bfloat16 [3072, 1024], P('sp', 'tp'), may hold values from -0.4375 to 0.4375
- w_out: bfloat16 [1024, 3072], P('tp', 'sp'), may hold values from -0.1875 to 0.1875
Outputs:
- mixed: bfloat16 [8192, 3072], P(('sp', 'tp'))
- row_lse: float32 [16, 8192], P('tp', 'sp')
All inputs are finite; a program needn't handle non-finite values.
Results may differ from a plain program's by a relative error of at most 0.014.
Values may be sent and summed in bfloat16 or wider, within the bound.
A program may use at most 64 MiB of HBM per device.

v0:
```python
from functools import partial

import jax
import jax.numpy as jnp
from jax import lax
from jax.sharding import PartitionSpec as P

HEAD_SIZE = 64
KEYS_BEHIND = 128


dilation_rates = (1, 4, 16)
neg_big = -1e30


def passed_along(block, axis, distance):
    devices = range(lax.axis_size(axis))
    route = [(i - distance, i) for i in devices if i - distance in devices]
    return lax.ppermute(block, axis, route)


def band(query_class_rows, key_class_rows, value_class_rows, key_first_index):
    sequence_length = query_class_rows.shape[0]
    if sequence_length <= KEYS_BEHIND:
        blocks = 1
        step = sequence_length
        q_blk = query_class_rows[None]
        k_blk = key_class_rows[None]
        v_blk = value_class_rows[None]
    else:
        blocks = sequence_length // KEYS_BEHIND
        step = KEYS_BEHIND
        q_blk = query_class_rows.reshape(blocks, KEYS_BEHIND, HEAD_SIZE)
        k_rows = key_class_rows.reshape(blocks + 1, KEYS_BEHIND, HEAD_SIZE)
        v_rows = value_class_rows.reshape(blocks + 1, KEYS_BEHIND, HEAD_SIZE)
        k_blk = jnp.concatenate([k_rows[:-1], k_rows[1:]], axis=1)
        v_blk = jnp.concatenate([v_rows[:-1], v_rows[1:]], axis=1)
    score = jnp.einsum(
        "nqd,nkd->nqk", q_blk, k_blk, preferred_element_type=jnp.float32
    ) * HEAD_SIZE ** (-0.5)
    row_at = jnp.arange(step, dtype=jnp.int32)[:, None]
    col_at = jnp.arange(k_blk.shape[1], dtype=jnp.int32)[None, :]
    dist = KEYS_BEHIND + row_at - col_at
    key_pos = (
        key_first_index + jnp.arange(blocks, dtype=jnp.int32)[:, None, None] * step + col_at[None]
    )
    mask = (dist >= 0) & (dist <= KEYS_BEHIND) & (key_pos >= 0)
    score = jnp.where(mask, score, neg_big)
    top = jnp.max(score, axis=-1, keepdims=True)
    weight = jnp.exp(score - top)
    denom = jnp.sum(weight, axis=-1)
    weight_bf = weight.astype(jnp.bfloat16)
    out = (
        jnp.einsum("nqk,nkd->nqd", weight_bf, v_blk, preferred_element_type=jnp.float32)
        / denom[..., None]
    )
    lse = top[..., 0] + jnp.log(denom)
    return (out.reshape(sequence_length, HEAD_SIZE), lse.reshape(sequence_length))


def shards(tokens, w_query, w_key, w_value, w_out):
    row_indices = tokens.shape[0]
    width = w_query.shape[1]
    head_outputs = width // HEAD_SIZE
    pieces = (
        lax.all_gather(w_query, "sp", axis=0, tiled=True),
        lax.all_gather(w_key, "sp", axis=0, tiled=True),
        lax.all_gather(w_value, "sp", axis=0, tiled=True),
    )
    q_sum, k_sum, v_sum = tuple(
        (jnp.dot(tokens, piece, preferred_element_type=jnp.float32) for piece in pieces)
    )
    query_input = q_sum.astype(jnp.bfloat16)
    keys = k_sum.astype(jnp.bfloat16)
    values = v_sum.astype(jnp.bfloat16)
    widest = KEYS_BEHIND * 16
    reach = (widest + row_indices - 1) // row_indices
    prior_keys, prior_values = passed_along((keys, values), "sp", 1)
    for level in range((reach - 1).bit_length()):
        far_keys, far_values = passed_along((prior_keys, prior_values), "sp", 1 << level)
        prior_keys = jnp.concatenate([far_keys, prior_keys], 0)
        prior_values = jnp.concatenate([far_values, prior_values], 0)
    base_offset = lax.axis_index("sp") * row_indices
    outs = []
    lses = []
    for dilation_rate in dilation_rates:
        window_keys = KEYS_BEHIND * dilation_rate
        sequence_length = row_indices // dilation_rate
        held = prior_keys.shape[0]
        key_all_rows = jnp.concatenate([prior_keys[held - window_keys :], keys], 0)
        value_all_rows = jnp.concatenate([prior_values[held - window_keys :], values], 0)
        query_class_rows = query_input.reshape(
            sequence_length, dilation_rate, head_outputs, HEAD_SIZE
        ).transpose(1, 2, 0, 3)
        key_class_rows = key_all_rows.reshape(
            KEYS_BEHIND + sequence_length, dilation_rate, head_outputs, HEAD_SIZE
        ).transpose(1, 2, 0, 3)
        value_class_rows = value_all_rows.reshape(
            KEYS_BEHIND + sequence_length, dilation_rate, head_outputs, HEAD_SIZE
        ).transpose(1, 2, 0, 3)
        key_first_index = base_offset // dilation_rate - KEYS_BEHIND
        banded = partial(band, key_first_index=key_first_index)
        out, lse = jax.vmap(jax.vmap(banded))(query_class_rows, key_class_rows, value_class_rows)
        outs.append(out.transpose(2, 0, 1, 3).reshape(row_indices, head_outputs, HEAD_SIZE))
        lses.append(lse.transpose(1, 2, 0).reshape(head_outputs, row_indices))
    lse_all = jnp.stack(lses, 0)
    peak = jnp.max(lse_all, axis=0)
    expo = jnp.exp(lse_all - peak)
    total = jnp.sum(expo, axis=0)
    mix = (expo / total).transpose(0, 2, 1)
    attended = jnp.sum(mix[..., None] * jnp.stack(outs, 0), axis=0)
    attended = attended.reshape(row_indices, width).astype(jnp.bfloat16)
    row_lse = peak + jnp.log(total)
    full_out = lax.all_gather(w_out, "sp", axis=1, tiled=True)
    mixed = lax.psum_scatter(
        jnp.dot(attended, full_out, preferred_element_type=jnp.float32).astype(jnp.bfloat16),
        "tp",
        scatter_dimension=0,
        tiled=True,
    )
    return (mixed, row_lse)


def solution(mesh):
    placed = (P("sp", None), P("sp", "tp"), P("sp", "tp"), P("sp", "tp"), P("tp", "sp"))
    return jax.shard_map(
        shards,
        mesh=mesh,
        in_specs=placed,
        out_specs=(P(("sp", "tp"), None), P("tp", "sp")),
        check_vma=False,
    )
```

profile of v0, /device:TPU:17, one launch (start us, length us, event | category | flops | bytes accessed | tf_op | source)
XLA Modules:
  0.0 392.1 jit_solution(13662421967980926335)
XLA Ops:
  10.4 68.0 %all-gather.7.cloned.1.call-done = bf16[3072,512]{1,0:T(8,128)(2,1)} async-done(((bf16[192,512]{1,0:T(8,128)(2,1)}), bf16[3072,512]{1,0:T(8,128)(2,1)}) %all-gather.7.cloned.1.call-update) | async-done | bytes 3145744 | tf_op jit(solution)/shard_map/all_gather | solution.py:67
  78.5 4.5 %convolution_convert_fusion.2 = bf16[512,512]{1,0:T(8,128)(2,1)} fusion(bf16[512,3072]{1,0:T(8,128)(2,1)S(1)} %copy-done, bf16[3072,512]{1,0:T(8,128)(2,1)} %all-gather.7.cloned.1.call-done), kind=kOutput, calls=%fused_computation.41 | convolution fusion | flops 1610874880 | bytes 6815744 | tf_op jit(solution)/shard_map/dot_general | solution.py:71
  83.0 3.1 collective-permute-start
  86.0 63.0 %all-gather.9.cloned.1.call-done = bf16[3072,512]{1,0:T(8,128)(2,1)} async-done(((bf16[192,512]{1,0:T(8,128)(2,1)}), bf16[3072,512]{1,0:T(8,128)(2,1)}) %all-gather.9.cloned.1.call-update) | async-done | bytes 3145744 | tf_op jit(solution)/shard_map/all_gather | solution.py:68
  149.0 4.5 %convolution_convert_fusion.1 = bf16[512,512]{1,0:T(8,128)(2,1)} fusion(bf16[512,3072]{1,0:T(8,128)(2,1)S(1)} %copy-done, bf16[3072,512]{1,0:T(8,128)(2,1)} %all-gather.9.cloned.1.call-done), kind=kOutput, calls=%fused_computation.40 | convolution fusion | flops 1610874880 | bytes 6815744 | tf_op jit(solution)/shard_map/dot_general | solution.py:71
  153.5 3.1 collective-permute-start.3
  156.6 63.0 %all-gather.5.cloned.1.call-done = bf16[3072,512]{1,0:T(8,128)(2,1)} async-done(((bf16[192,512]{1,0:T(8,128)(2,1)}), bf16[3072,512]{1,0:T(8,128)(2,1)}) %all-gather.5.cloned.1.call-update) | async-done | bytes 3145744 | tf_op jit(solution)/shard_map/all_gather | solution.py:66
  219.6 4.5 %convolution_convert_fusion.3 = bf16[512,512]{0,1:T(8,128)(2,1)} fusion(bf16[512,3072]{1,0:T(8,128)(2,1)S(1)} %copy-done, bf16[3072,512]{1,0:T(8,128)(2,1)} %all-gather.5.cloned.1.call-done), kind=kOutput, calls=%fused_computation.42 | convolution fusion | flops 1610874880 | bytes 6815744 | tf_op jit(solution)/shard_map/dot_general | solution.py:71
  237.5 2.5 fusion.4
  243.6 3.3 collective-permute-start.1
  247.1 3.2 fusion.49
  252.4 3.1 collective-permute-start.4
  255.5 13.2 %collective-permute-done.1 = bf16[512,512]{1,0:T(8,128)(2,1)S(1)} collective-permute-done((bf16[512,512]{1,0:T(8,128)(2,1)}, bf16[512,512]{1,0:T(8,128)(2,1)S(1)}, u32[]{:S(2)}, u32[]{:S(2)}) %collective-permute-start.1) | collective-permute-done | bytes 524320 | tf_op jit(solution)/shard_map/ppermute | solution.py:19
  268.7 2.7 pad_maximum_fusion.2
  276.1 2.2 fusion.5
  278.3 1.9 copy-done.3
  282.3 4.5 %collective-permute-done.4 = bf16[512,512]{1,0:T(8,128)(2,1)} collective-permute-done((bf16[512,512]{1,0:T(8,128)(2,1)}, bf16[512,512]{1,0:T(8,128)(2,1)}, u32[]{:S(2)}, u32[]{:S(2)}) %collective-permute-start.4) | collective-permute-done | bytes 524320 | tf_op jit(solution)/shard_map/ppermute | solution.py:19
  286.8 2.7 pad_maximum_fusion.4
  292.2 4.4 %fusion.44 = f32[128,4,8,64]{0,3,2,1:T(8,128)} fusion(bf16[256,4,8,64]{0,3,2,1:T(8,128)(2,1)S(1)} %copy.96, f32[4,8,128,256]{3,2,1,0:T(8,128)} %copy-done.3, f32[4,8,128]{2,1,0:T(8,128)S(1)} %get-tuple-element.18, pred[128,256]{1,0:T(8,128)(4,1)S(1)} %get-tuple-element.15, f32[128,4,8]{0,2,1:T(8,128)S(1)} %bitcast.107), kind=kOutput, calls=%fused_computation.59 | convolution fusion | flops 138674176 | bytes 6356992 | tf_op jit(solution)/shard_map/vmap(vmap(nqk,nkd->nqd))/dot_general | solution.py:54
  296.6 3.1 copy.97
  301.5 2.1 collective-permute-start.5
  303.6 10.7 %collective-permute-done.2 = bf16[1024,512]{1,0:T(8,128)(2,1)} collective-permute-done((bf16[1024,512]{1,0:T(8,128)(2,1)}, bf16[1024,512]{1,0:T(8,128)(2,1)}, u32[]{:S(2)}, u32[]{:S(2)}) %collective-permute-start.2) | collective-permute-done | bytes 1048608 | tf_op jit(solution)/shard_map/ppermute | solution.py:19
  316.0 4.5 %reshape.351 = bf16[160,16,8,64]{3,2,1,0:T(8,128)(2,1)} reshape(bf16[2560,512]{1,0:T(8,128)(2,1)S(1)} %pad_maximum_fusion) | data formatting | bytes 5242880 | tf_op jit(solution)/shard_map/reshape | solution.py:95
  320.5 8.8 %copy.85 = bf16[160,16,8,64]{0,3,2,1:T(8,128)(2,1)} copy(bf16[160,16,8,64]{3,2,1,0:T(8,128)(2,1)} %reshape.351) | data formatting | bytes 5242880 | tf_op jit(solution)/shard_map/reshape | solution.py:95
  329.3 3.6 fusion.6
  332.9 2.0 copy-done.2
  338.6 4.5 %reshape.357 = bf16[160,16,8,64]{3,2,1,0:T(8,128)(2,1)} reshape(bf16[2560,512]{1,0:T(8,128)(2,1)S(1)} %pad_maximum_fusion.1) | data formatting | bytes 5242880 | tf_op jit(solution)/shard_map/reshape | solution.py:98
  343.2 8.6 %copy.98 = bf16[160,16,8,64]{0,3,2,1:T(8,128)(2,1)} copy(bf16[160,16,8,64]{3,2,1,0:T(8,128)(2,1)} %reshape.357) | data formatting | bytes 5242880 | tf_op jit(solution)/shard_map/reshape | solution.py:98
  351.8 4.3 %bitcast_divide_fusion = f32[32,16,8,64]{3,0,2,1:T(8,128)S(1)} fusion(f32[32,16,8]{0,2,1:T(8,128)S(1)} %bitcast.104, bf16[160,16,8,64]{0,3,2,1:T(8,128)(2,1)} %copy.98, f32[16,8,32,160]{3,2,1,0:T(8,128)} %copy-done.2, f32[16,8,32]{2,1,0:T(8,128)S(1)} %get-tuple-element.16, pred[32,160]{1,0:T(8,128)(4,1)S(1)} %fusion.64), kind=kOutput, calls=%fused_computation.26 | convolution fusion | flops 86769664 | bytes 6329344 | tf_op jit(solution)/shard_map/vmap(vmap(nqk,nkd->nqd))/dot_general | solution.py:54
  359.1 3.0 fusion.13
  362.0 5.7 %convolution_convert_fusion = bf16[512,3072]{1,0:T(8,128)(2,1)} fusion(bf16[512,512]{0,1:T(8,128)(2,1)} %bitcast.103, bf16[512,3072]{0,1:T(8,128)(2,1)} %all-gather.11.cloned.1.call-done), kind=kOutput, calls=%fused_computation | convolution fusion | flops 1612185600 | bytes 6815744 | tf_op jit(solution)/shard_map/dot_general | solution.py:116
  368.4 17.2 %reduce-scatter.2.cloned.1.call-done = bf16[256,3072]{1,0:T(8,128)(2,1)} async-done(((bf16[512,3072]{1,0:T(8,128)(2,1)}), bf16[256,3072]{1,0:T(8,128)(2,1)}) %reduce-scatter.2.cloned.1.call-update) | async-done | bytes 1572880 | tf_op jit(solution)/shard_map/reduce_scatter | solution.py:115
  (88 shorter events, 42.5 us)
Async XLA Ops:
  7.2 71.3 %copy-start = (bf16[512,3072]{1,0:T(8,128)(2,1)S(1)}, bf16[512,3072]{1,0:T(8,128)(2,1)}, u32[]{:S(2)}) copy-start(bf16[512,3072]{1,0:T(8,128)(2,1)} %param.5) | copy-start | bytes 9437188
  7.2 71.3 %all-gather.7.cloned.1.call-start = ((), (), s32[]{:S(2)}) async-start(), calls=%async_computation.2 | async-start | bytes 3342336 | tf_op jit(solution)/shard_map/all_gather | solution.py:67
  7.9 141.1 %all-gather.9.cloned.1.call-start = ((), (), s32[]{:S(2)}) async-start(), calls=%async_computation.3 | async-start | bytes 3342336 | tf_op jit(solution)/shard_map/all_gather | solution.py:68
  8.7 210.9 %all-gather.5.cloned.1.call-start = ((), (), s32[]{:S(2)}) async-start(), calls=%async_computation.1 | async-start | bytes 3342336 | tf_op jit(solution)/shard_map/all_gather | solution.py:66
  9.4 352.6 %all-gather.11.cloned.1.call-start = ((), (), s32[]{:S(2)}) async-start(), calls=%async_computation.4 | async-start | bytes 3342336 | tf_op jit(solution)/shard_map/all_gather | solution.py:114
  10.0 375.6 %reduce-scatter.2.cloned.1.call-start = ((), (), s32[]{:S(2)}) async-start(), calls=%async_computation.5 | async-start | bytes 4718592 | tf_op jit(solution)/shard_map/reduce_scatter | solution.py:115
  83.0 145.6 %collective-permute-start = (bf16[512,512]{1,0:T(8,128)(2,1)}, bf16[512,512]{1,0:T(8,128)(2,1)}, u32[]{:S(2)}, u32[]{:S(2)}) collective-permute-start(bf16[512,512]{1,0:T(8,128)(2,1)} %convolution_convert_fusion.2), channel_id=1, source_target_pairs={{0,2},{2,4},{4,6},{6,8},{8,10},{10,12},{12,14},{14,16},{16,18},{18... | collective-permute-start | bytes 1572872 | tf_op jit(solution)/shard_map/ppermute | solution.py:19
  153.5 80.5 %collective-permute-start.3 = (bf16[512,512]{1,0:T(8,128)(2,1)}, bf16[512,512]{1,0:T(8,128)(2,1)}, u32[]{:S(2)}, u32[]{:S(2)}) collective-permute-start(bf16[512,512]{1,0:T(8,128)(2,1)} %convolution_convert_fusion.1), channel_id=1, source_target_pairs={{0,2},{2,4},{4,6},{6,8},{8,10},{10,12},{12,14},{14,16},{16,18},{18... | collective-permute-start | bytes 1572872 | tf_op jit(solution)/shard_map/ppermute | solution.py:19
  224.1 4.4 %copy-start.9 = (bf16[512,512]{0,1:T(8,128)(2,1)S(1)}, bf16[512,512]{0,1:T(8,128)(2,1)}, u32[]{:S(2)}) copy-start(bf16[512,512]{0,1:T(8,128)(2,1)} %convolution_convert_fusion.3) | copy-start | bytes 1572868
  240.0 2.0 copy-start.5
  243.6 25.1 %collective-permute-start.1 = (bf16[512,512]{1,0:T(8,128)(2,1)}, bf16[512,512]{1,0:T(8,128)(2,1)S(1)}, u32[]{:S(2)}, u32[]{:S(2)}) collective-permute-start(bf16[512,512]{1,0:T(8,128)(2,1)} %collective-permute-done), channel_id=1, source_target_pairs={{0,2},{2,4},{4,6},{6,8},{8,10},{10,12},{12,14},{14,16},{16,18},{18... | collective-permute-start | bytes 1572872 | tf_op jit(solution)/shard_map/ppermute | solution.py:19
  252.4 34.4 %collective-permute-start.4 = (bf16[512,512]{1,0:T(8,128)(2,1)}, bf16[512,512]{1,0:T(8,128)(2,1)}, u32[]{:S(2)}, u32[]{:S(2)}) collective-permute-start(bf16[512,512]{1,0:T(8,128)(2,1)} %collective-permute-done.3), channel_id=1, source_target_pairs={{0,2},{2,4},{4,6},{6,8},{8,10},{10,12},{12,14},{14,16},{16,18},{18... | collective-permute-start | bytes 1572872 | tf_op jit(solution)/shard_map/ppermute | solution.py:19
  268.7 4.6 %copy-start.7 = (bf16[512,512]{1,0:T(8,128)(2,1)}, bf16[512,512]{1,0:T(8,128)(2,1)S(1)}, u32[]{:S(2)}) copy-start(bf16[512,512]{1,0:T(8,128)(2,1)S(1)} %collective-permute-done.1) | copy-start | bytes 1572868
  271.4 43.0 %collective-permute-start.2 = (bf16[1024,512]{1,0:T(8,128)(2,1)}, bf16[1024,512]{1,0:T(8,128)(2,1)}, u32[]{:S(2)}, u32[]{:S(2)}) collective-permute-start(bf16[1024,512]{1,0:T(8,128)(2,1)} %get-tuple-element.11), channel_id=1, source_target_pairs={{0,4},{2,6},{4,8},{6,10},{8,12},{10,14},{12,16},{14,18},{16,20},{1... | collective-permute-start | bytes 3145736 | tf_op jit(solution)/shard_map/ppermute | solution.py:19
  278.3 2.0 copy-start.3
  296.6 17.7 %copy-start.8 = (bf16[512,512]{1,0:T(8,128)(2,1)S(1)}, bf16[512,512]{1,0:T(8,128)(2,1)}, u32[]{:S(2)}) copy-start(bf16[512,512]{1,0:T(8,128)(2,1)} %copy-done.7) | copy-start | bytes 1572868
  301.5 35.3 %collective-permute-start.5 = (bf16[1024,512]{1,0:T(8,128)(2,1)}, bf16[1024,512]{1,0:T(8,128)(2,1)}, u32[]{:S(2)}, u32[]{:S(2)}) collective-permute-start(bf16[1024,512]{1,0:T(8,128)(2,1)} %get-tuple-element.13), channel_id=1, source_target_pairs={{0,4},{2,6},{4,8},{6,10},{8,12},{10,14},{12,16},{14,18},{16,20},{1... | collective-permute-start | bytes 3145736 | tf_op jit(solution)/shard_map/ppermute | solution.py:19
  320.5 8.8 %copy-start.6 = (bf16[32,16,8,64]{3,2,1,0:T(8,128)(2,1)S(1)}, bf16[32,16,8,64]{3,2,1,0:T(8,128)(2,1)}, u32[]{:S(2)}) copy-start(bf16[32,16,8,64]{3,2,1,0:T(8,128)(2,1)} %reshape.350) | copy-start | bytes 1572868
  332.9 2.0 copy-start.2
  356.1 3.0 copy-start.4
  362.0 23.5 %copy-start.1 = (bf16[512,3072]{1,0:T(8,128)(2,1)S(1)}, bf16[512,3072]{1,0:T(8,128)(2,1)}, u32[]{:S(2)}) copy-start(bf16[512,3072]{1,0:T(8,128)(2,1)} %param.5) | copy-start | bytes 9437188
Sparse Core Ops, SparseCore 0:
  10.8 67.6 all-gather.6
  81.2 67.7 all-gather.8
  151.8 67.7 all-gather.4
  222.2 96.1 all-gather.10
  367.9 17.6 reduce-scatter.1
where the time goes:
time: 394 us; the launch traced here: 392 us
  waiting for transfers between devices  242 us (61%)
  local copies, waits for them, and re-layouts  59.9 us (15%)
  matrix products  39.2 us (10%)
  other arithmetic  19.8 us (5%)
  starting transfers between devices  16.8 us (4%)
  between operations  14.2 us (4%)
    all_gather x1, waiting for transfers between devices, shards(): lax.all_gather(w_key, 'sp', axis=0, tiled=True)  68 us
    all_gather x1, waiting for transfers between devices, shards(): lax.all_gather(w_query, 'sp', axis=0, tiled=True)  63 us
    all_gather x1, waiting for transfers between devices, shards(): lax.all_gather(w_value, 'sp', axis=0, tiled=True)  63 us
    ppermute x6, waiting for transfers between devices, passed_along(): return lax.ppermute(block, axis, route)  28.5 us
    reduce_scatter x1, waiting for transfers between devices, shards(): lax.psum_scatter(jnp.dot(attended, full_out, preferred_element_type=jnp.f...  17.2 us
    ppermute x6, starting transfers between devices, passed_along(): return lax.ppermute(block, axis, route)  16.6 us
    reshape x4, local copies, waits for them, and re-layouts, shards(): key_all_rows.reshape(KEYS_BEHIND + sequence_length, dilation_rate, head_o...  16.1 us
    reshape x4, local copies, waits for them, and re-layouts, shards(): value_all_rows.reshape(KEYS_BEHIND + sequence_length, dilation_rate, head...  16 us
  transfers between devices with their start and end apart: 11, of which 7 were waited for; matrix products, arithmetic and copies ran while one was open for 27% of the time, Pallas kernels for 0%

commit v1 on v0

v1 whole, which is shorter than its diff:
```python
import functools

import jax
import jax.numpy as jnp
from jax import lax
from jax.experimental import pallas as pl
from jax.experimental.pallas import tpu as pltpu
from jax.sharding import PartitionSpec as P

HEAD_SIZE = 64
KEYS_BEHIND = 128
LANES = 128

dilation_rates = (1, 4, 16)
neg_big = -1e30

MESH = pl.DeviceIdType.MESH
VMEM = pltpu.VMEM


def at(sp, tp):
    return {"sp": sp, "tp": tp}


def project_kernel(
    n, n_tp, group, far, w_ref, tok_ref, q_ref, kv_ref, halo_ref,
    tok_all, w_all, w1_send, w1_recv, w2_send, w2_recv,
    t_send, t_recv, d_send, d_recv, f_send, f_recv, h_send, h_recv, own_sem,
):
    sp, tp = lax.axis_index("sp"), lax.axis_index("tp")
    planes = n // group
    g, plane = lax.rem(sp, group), sp // group
    rows = tok_ref.shape[0]
    part = rows // n_tp
    half = part // 2

    barrier = pltpu.get_barrier_semaphore()

    def greet(j, _):
        pl.semaphore_signal(barrier, inc=1, device_id=at(lax.rem(sp + j, n), tp), device_id_type=MESH)
        return _

    lax.fori_loop(1, n, greet, 0)
    for j in range(1, n_tp):
        pl.semaphore_signal(barrier, inc=1, device_id=at(sp, lax.rem(tp + j, n_tp)), device_id_type=MESH)

    own_t = pltpu.make_async_copy(tok_ref, tok_all.at[g], own_sem.at[0])
    own_w = pltpu.make_async_copy(w_ref.at[g], w_all.at[sp], own_sem.at[1])
    own_t.start()
    own_w.start()
    pl.semaphore_wait(barrier, n - 1 + n_tp - 1)

    def mate(i):
        return plane * group + (g ^ i)

    def w_in_plane(i):
        return pltpu.make_async_remote_copy(
            src_ref=w_ref.at[g ^ i], dst_ref=w_all.at[sp], send_sem=w1_send.at[i], recv_sem=w1_recv.at[i],
            device_id=at(mate(i), tp), device_id_type=MESH)

    def w_in_plane_arrives(i):
        return pltpu.make_async_remote_copy(
            src_ref=w_ref.at[g ^ i], dst_ref=w_all.at[mate(i)], send_sem=w1_send.at[i], recv_sem=w1_recv.at[i],
            device_id=at(mate(i), tp), device_id_type=MESH)

    def w_to_plane(i, k):
        source = w_ref.at[g] if i == 0 else w_all.at[mate(i)]
        return pltpu.make_async_remote_copy(
            src_ref=source, dst_ref=w_all.at[mate(i)],
            send_sem=w2_send.at[i, k], recv_sem=w2_recv.at[i, k],
            device_id=at(lax.rem(sp + k * group, n), tp), device_id_type=MESH)

    def w_to_plane_arrives(i, k):
        origin = lax.rem(plane + planes - k, planes) * group + (g ^ i)
        return pltpu.make_async_remote_copy(
            src_ref=w_ref.at[g], dst_ref=w_all.at[origin],
            send_sem=w2_send.at[i, k], recv_sem=w2_recv.at[i, k],
            device_id=at(lax.rem(sp + k * group, n), tp), device_id_type=MESH)

    mine = pl.ds(pl.multiple_of(tp * part, part), part)

    def halves(k):
        return pl.ds(pl.multiple_of(tp * part + k * half, half), half)

    def tokens_out(i):
        return pltpu.make_async_remote_copy(
            src_ref=tok_ref.at[mine], dst_ref=tok_all.at[g, mine], send_sem=t_send.at[i], recv_sem=t_recv.at[i],
            device_id=at(mate(i), tp), device_id_type=MESH)

    def tokens_in(i):
        return pltpu.make_async_remote_copy(
            src_ref=tok_ref.at[mine], dst_ref=tok_all.at[g ^ i, mine], send_sem=t_send.at[i], recv_sem=t_recv.at[i],
            device_id=at(mate(i), tp), device_id_type=MESH)

    def corner_out(i):
        ref = tok_all.at[g ^ i, halves(i - 1)]
        return pltpu.make_async_remote_copy(
            src_ref=ref, dst_ref=ref, send_sem=d_send.at[i], recv_sem=d_recv.at[i],
            device_id=at(mate(3 - i), tp), device_id_type=MESH)

    def corner_in(i):
        ref = tok_all.at[g ^ 3, halves(i - 1)]
        return pltpu.make_async_remote_copy(
            src_ref=ref, dst_ref=ref, send_sem=d_send.at[i], recv_sem=d_recv.at[i],
            device_id=at(mate(3 - i), tp), device_id_type=MESH)

    def across(i, j):
        ref = tok_all.at[g ^ i, mine]
        return pltpu.make_async_remote_copy(
            src_ref=ref, dst_ref=ref, send_sem=f_send.at[i, j], recv_sem=f_recv.at[i, j],
            device_id=at(sp, lax.rem(tp + j, n_tp)), device_id_type=MESH)

    def across_in(i, j):
        origin = lax.rem(tp + n_tp - j, n_tp)
        ref = tok_all.at[g ^ i, pl.ds(pl.multiple_of(origin * part, part), part)]
        return pltpu.make_async_remote_copy(
            src_ref=ref, dst_ref=ref, send_sem=f_send.at[i, j], recv_sem=f_recv.at[i, j],
            device_id=at(sp, lax.rem(tp + j, n_tp)), device_id_type=MESH)

    near = [i for i in (1, 2) if i < group]
    for i in range(1, group):
        w_in_plane(i).start()
    if planes > 1:
        lax.fori_loop(1, planes, lambda k, _: (w_to_plane(0, k).start(), _)[1], 0)
    for i in near:
        tokens_out(i).start()
    for i in range(1, group):
        w_in_plane_arrives(i).wait_recv()
        if planes > 1:
            lax.fori_loop(1, planes, lambda k, _, i=i: (w_to_plane(i, k).start(), _)[1], 0)
    for i in near:
        tokens_in(i).wait_recv()
        if group == 4:
            corner_out(i).start()
        for j in range(1, n_tp):
            across(i, j).start()

    own_w.wait()
    own_t.wait()
    for i in range(group):
        if planes > 1:
            lax.fori_loop(1, planes, lambda k, _, i=i: (w_to_plane_arrives(i, k).wait_recv(), _)[1], 0)

    def halo_block(h, b):
        view = pl.ds(pl.multiple_of(b * rows, rows), rows)
        return view

    def halo_out(h, i):
        view = pl.ds(pl.multiple_of((g ^ i) * rows, rows), rows)
        return pltpu.make_async_remote_copy(
            src_ref=kv_ref.at[view], dst_ref=halo_ref.at[far - h, view],
            send_sem=h_send.at[h, i], recv_sem=h_recv.at[h, i],
            device_id=at(lax.rem(sp + h * group, n), tp), device_id_type=MESH)

    tile = min(256, rows)

    for i in range(group):
        if i == 3:
            for k in (1, 2):
                corner_in(k).wait_recv()
            for j in range(1, n_tp):
                across(i, j).start()
        if i > 0:
            for j in range(1, n_tp):
                across_in(i, j).wait_recv()
        block = g ^ i

        def one(s, _, block=block):
            x = tok_all[block, pl.ds(pl.multiple_of(s * tile, tile), tile), :]
            w = w_all[...].reshape(-1, 3 * LANES)
            y = jnp.dot(x, w, preferred_element_type=jnp.float32).astype(jnp.bfloat16)
            to = pl.ds(pl.multiple_of(block * rows + s * tile, tile), tile)
            q_ref[to, :] = y[:, :LANES]
            kv_ref[to, :] = y[:, LANES:]
            return _

        lax.fori_loop(0, rows // tile, one, 0)
        for h in range(1, far + 1):
            @pl.when(plane + h < planes)
            def _():
                halo_out(h, i).start()

    for h in range(1, far + 1):
        @pl.when(plane - h >= 0)
        def _():
            for i in range(group):
                halo_out(h, i).wait_recv()

        @pl.when(plane - h < 0)
        def _():
            halo_ref[far - h] = jnp.zeros(halo_ref.shape[1:], halo_ref.dtype)

        @pl.when(plane + h < planes)
        def _():
            for i in range(group):
                halo_out(h, i).wait_send()

    for i in range(1, group):
        w_in_plane(i).wait_send()
        for j in range(1, n_tp):
            across(i, j).wait_send()
    for i in near:
        tokens_out(i).wait_send()
        if group == 4:
            corner_out(i).wait_send()
    if planes > 1:
        for i in range(group):
            lax.fori_loop(1, planes, lambda k, _, i=i: (w_to_plane(i, k).wait_send(), _)[1], 0)


def attend_kernel(heads, base_ref, q_ref, kv_ref, halo_ref, att_ref, lse_ref, qs, ks, vs, top_s, den_s, acc_s):
    base = base_ref[0]
    own = q_ref.shape[0]
    behind = ks.shape[0] - own
    pieces, piece_rows = halo_ref.shape[0], halo_ref.shape[1]
    qs[...] = q_ref[...].astype(jnp.float32) * HEAD_SIZE ** (-0.5)
    for h in range(pieces):
        ks[h * piece_rows : (h + 1) * piece_rows] = halo_ref[h, :, :LANES].astype(jnp.float32)
        vs[h * piece_rows : (h + 1) * piece_rows] = halo_ref[h, :, LANES:].astype(jnp.float32)
    ks[behind:] = kv_ref[:, :LANES].astype(jnp.float32)
    vs[behind:] = kv_ref[:, LANES:].astype(jnp.float32)

    for number, d in enumerate(dilation_rates):
        step = min(KEYS_BEHIND, own // d)
        count = own // d // step
        span = step + KEYS_BEHIND

        def block(index, _, number=number, d=d, step=step, span=span):
            cls, b = lax.rem(index, d), index // d
            start = b * (step * d) + cls
            q_at = pl.ds(start, step, stride=d) if d > 1 else pl.ds(pl.multiple_of(start, step), step)
            k_start = behind - KEYS_BEHIND * d + start
            k_at = pl.ds(k_start, span, stride=d) if d > 1 else pl.ds(pl.multiple_of(k_start, step), span)
            q = qs[q_at, :]
            k = ks[k_at, :].astype(jnp.bfloat16)
            v = vs[k_at, :].astype(jnp.bfloat16)
            low = lax.broadcasted_iota(jnp.int32, (step, LANES), 1) < HEAD_SIZE
            q2 = jnp.concatenate([jnp.where(low, q, 0.0), jnp.where(low, 0.0, q)], axis=0).astype(jnp.bfloat16)
            s = lax.dot_general(q2, k, (((1,), (1,)), ((), ())), preferred_element_type=jnp.float32)
            row = lax.broadcasted_iota(jnp.int32, (step, span), 0)
            col = lax.broadcasted_iota(jnp.int32, (step, span), 1)
            dist = KEYS_BEHIND + row - col
            first = base // d + b * step - KEYS_BEHIND
            seen = (dist >= 0) & (dist <= KEYS_BEHIND) & (first + col >= 0)
            s = jnp.where(jnp.concatenate([seen, seen], axis=0), s, neg_big)
            top = jnp.max(s, axis=1, keepdims=True)
            p = jnp.exp(s - top)
            den = jnp.sum(p, axis=1, keepdims=True)
            o = jnp.dot(p.astype(jnp.bfloat16), v, preferred_element_type=jnp.float32)
            top = jnp.where(low, top[:step], top[step:])
            den = jnp.where(low, den[:step], den[step:])
            o = jnp.where(low, o[:step], o[step:])
            if number == 0:
                top_s[q_at, :] = top
                den_s[q_at, :] = den
                acc_s[q_at, :] = o
            else:
                was = top_s[q_at, :]
                new = jnp.maximum(was, top)
                old_scale, scale = jnp.exp(was - new), jnp.exp(top - new)
                top_s[q_at, :] = new
                den_s[q_at, :] = den_s[q_at, :] * old_scale + den * scale
                acc_s[q_at, :] = acc_s[q_at, :] * old_scale + o * scale
            return _

        lax.fori_loop(0, d * count, block, 0, unroll=2)

    rows = lse_ref.shape[2]
    att_ref[...] = (acc_s[...] / den_s[...]).astype(jnp.bfloat16)
    for t in range(own // LANES):
        at_rows = pl.ds(t * LANES, LANES)
        lse = (top_s[at_rows, :] + jnp.log(den_s[at_rows, :])).T
        b, off = (t * LANES) // rows, (t * LANES) % rows
        for h in range(heads):
            lse_ref[b, h : h + 1, off : off + LANES] = lse[h * HEAD_SIZE : h * HEAD_SIZE + 1, :]


def return_kernel(n_tp, group, att_ref, lse_ref, all_ref, lse_all, a_send, a_recv, l_send, l_recv, own_sem):
    sp, tp = lax.axis_index("sp"), lax.axis_index("tp")
    g, plane = lax.rem(sp, group), sp // group
    part = all_ref.shape[0]
    width = all_ref.shape[1] // n_tp
    others = [(i, j) for i in range(group) for j in range(n_tp) if (i, j) != (0, 0)]

    def device(i, j):
        return plane * group + (g ^ i), lax.rem(tp + j, n_tp)

    barrier = pltpu.get_barrier_semaphore()
    for i, j in others:
        pl.semaphore_signal(barrier, inc=1, device_id=at(*device(i, j)), device_id_type=MESH)

    def columns(h, c):
        return pl.ds(pl.multiple_of(c * width + h * LANES, LANES), LANES)

    def sent_rows(i, j):
        c = lax.rem(tp + j, n_tp)
        return pl.ds(pl.multiple_of((g ^ i) * (part * n_tp) + c * part, part), part)

    own = pltpu.make_async_copy(att_ref.at[sent_rows(0, 0)], all_ref.at[:, columns(g, tp)], own_sem.at[0])
    own_l = pltpu.make_async_copy(lse_ref.at[g], lse_all.at[g], own_sem.at[1])
    own.start()
    own_l.start()
    pl.semaphore_wait(barrier, len(others))

    def out(i, j):
        return pltpu.make_async_remote_copy(
            src_ref=att_ref.at[sent_rows(i, j)], dst_ref=all_ref.at[:, columns(g, tp)],
            send_sem=a_send.at[i, j], recv_sem=a_recv.at[i, j], device_id=at(*device(i, j)), device_id_type=MESH)

    def arrives(i, j):
        return pltpu.make_async_remote_copy(
            src_ref=att_ref.at[sent_rows(i, j)],
            dst_ref=all_ref.at[:, columns(g ^ i, lax.rem(tp + n_tp - j, n_tp))],
            send_sem=a_send.at[i, j], recv_sem=a_recv.at[i, j], device_id=at(*device(i, j)), device_id_type=MESH)

    def lse_out(i):
        return pltpu.make_async_remote_copy(
            src_ref=lse_ref.at[g ^ i], dst_ref=lse_all.at[g], send_sem=l_send.at[i], recv_sem=l_recv.at[i],
            device_id=at(*device(i, 0)), device_id_type=MESH)

    def lse_in(i):
        return pltpu.make_async_remote_copy(
            src_ref=lse_ref.at[g ^ i], dst_ref=lse_all.at[g ^ i], send_sem=l_send.at[i], recv_sem=l_recv.at[i],
            device_id=at(*device(i, 0)), device_id_type=MESH)

    for i, j in others:
        out(i, j).start()
    for i in range(1, group):
        lse_out(i).start()
    own.wait()
    own_l.wait()
    for i, j in others:
        arrives(i, j).wait_recv()
    for i in range(1, group):
        lse_in(i).wait_recv()
    for i, j in others:
        out(i, j).wait_send()
    for i in range(1, group):
        lse_out(i).wait_send()


def shards(n, n_tp, tokens, w_query, w_key, w_value, w_out):
    rows, model = tokens.shape
    depth, width = w_query.shape
    slabs = width // LANES
    reach = KEYS_BEHIND * dilation_rates[-1]
    group = 1
    while group < 4 and group * rows < reach and slabs % (2 * group) == 0 and n % (2 * group) == 0:
        group *= 2
    assert slabs == group
    far = (reach + group * rows - 1) // (group * rows)
    planes = n // group
    own = group * rows
    part = rows // n_tp
    heads = LANES // HEAD_SIZE

    full_out = lax.all_gather(w_out, "sp", axis=1, tiled=True)
    full_out = lax.all_gather(full_out, "tp", axis=0, tiled=True)

    w = jnp.stack([w_query, w_key, w_value], 1).reshape(depth, 3, group, LANES)
    w = w.transpose(2, 0, 1, 3).reshape(group, depth, 3 * LANES)

    dma = pltpu.SemaphoreType.DMA
    vmem = pl.BlockSpec(memory_space=VMEM)
    q, kv, halo = pl.pallas_call(
        functools.partial(project_kernel, n, n_tp, group, far),
        out_shape=(
            jax.ShapeDtypeStruct((own, LANES), jnp.bfloat16),
            jax.ShapeDtypeStruct((own, 2 * LANES), jnp.bfloat16),
            jax.ShapeDtypeStruct((far, own, 2 * LANES), jnp.bfloat16),
        ),
        in_specs=[vmem, pl.BlockSpec(memory_space=pl.ANY)],
        out_specs=(vmem, vmem, vmem),
        scratch_shapes=[
            VMEM((group, rows, model), jnp.bfloat16),
            VMEM((n, depth, 3 * LANES), jnp.bfloat16),
            dma((group,)), dma((group,)),
            dma((group, planes)), dma((group, planes)),
            dma((group,)), dma((group,)),
            dma((group,)), dma((group,)),
            dma((group, n_tp)), dma((group, n_tp)),
            dma((far + 1, group)), dma((far + 1, group)),
            dma((2,)),
        ],
        compiler_params=pltpu.CompilerParams(collective_id=0, has_side_effects=True, vmem_limit_bytes=48 << 20),
        cost_estimate=pl.CostEstimate(flops=2 * own * model * 3 * LANES, bytes_accessed=1 << 24, transcendentals=0),
        name="project",
    )(w, tokens)

    base = (lax.axis_index("sp") // group * own).astype(jnp.int32).reshape(1)
    behind = far * own
    f32 = jnp.float32
    att, lse = pl.pallas_call(
        functools.partial(attend_kernel, heads),
        out_shape=(
            jax.ShapeDtypeStruct((own, LANES), jnp.bfloat16),
            jax.ShapeDtypeStruct((group, heads, rows), f32),
        ),
        in_specs=[pl.BlockSpec(memory_space=pltpu.SMEM), vmem, vmem, vmem],
        out_specs=(vmem, vmem),
        scratch_shapes=[
            VMEM((own, LANES), f32), VMEM((behind + own, LANES), f32), VMEM((behind + own, LANES), f32),
            VMEM((own, LANES), f32), VMEM((own, LANES), f32), VMEM((own, LANES), f32),
        ],
        compiler_params=pltpu.CompilerParams(vmem_limit_bytes=32 << 20),
        cost_estimate=pl.CostEstimate(flops=1 << 32, bytes_accessed=1 << 22, transcendentals=1 << 22),
        name="attend",
    )(base, q, kv, halo)

    attended, lse_all = pl.pallas_call(
        functools.partial(return_kernel, n_tp, group),
        out_shape=(
            jax.ShapeDtypeStruct((part, n_tp * width), jnp.bfloat16),
            jax.ShapeDtypeStruct((group, heads, rows), f32),
        ),
        in_specs=[vmem, vmem],
        out_specs=(vmem, vmem),
        scratch_shapes=[
            dma((group, n_tp)), dma((group, n_tp)), dma((group,)), dma((group,)), dma((2,)),
        ],
        compiler_params=pltpu.CompilerParams(collective_id=1, has_side_effects=True),
        name="hand_back",
    )(att, lse)

    mixed = jnp.dot(attended, full_out, preferred_element_type=f32).astype(jnp.bfloat16)
    return mixed, lse_all.reshape(group * heads, rows)


def solution(mesh):
    placed = (P("sp", None), P("sp", "tp"), P("sp", "tp"), P("sp", "tp"), P("tp", "sp"))
    return jax.shard_map(
        functools.partial(shards, mesh.shape["sp"], mesh.shape["tp"]),
        mesh=mesh,
        in_specs=placed,
        out_specs=(P(("sp", "tp"), None), P("tp", "sp")),
        check_vma=False,
    )
```

time: 394 us -> 209 us (0.53)
  waiting for transfers between devices: 242 us -> 71.2 us
  Pallas kernels: 0 us -> 111 us
  local copies, waits for them, and re-layouts: 59.9 us -> 4.36 us
  matrix products: 39.2 us -> 5.94 us
  other arithmetic: 19.8 us -> 1.36 us
  starting transfers between devices: 16.8 us -> 0.08 us
    all_gather x3 -> x1, waiting for transfers between devices: 194 us -> 0.01 us  [shards(): full_out = lax.all_gather(full_out, 'tp', axis=0, tiled=True)]
    pallas_call x0 -> x3, Pallas kernels: none -> 111 us  [the longest x1 79.2 us: shards(): pl.pallas_call(functools.partial(project_kernel, n, n_tp, group, far), ou...]
    all_gather x1, waiting for transfers between devices: 0.01 us -> 70.5 us  [shards(): full_out = lax.all_gather(w_out, 'sp', axis=1, tiled=True)]
    reshape x13 -> x2, local copies, waits for them, and re-layouts: 38 us -> 1.88 us  [the longest x1 1.34 us: shards(): return (mixed, lse_all.reshape(group * heads, rows))]
    dot_general x10 -> x1, matrix products: 39.2 us -> 5.94 us  [shards(): jnp.dot(attended, full_out, preferred_element_type=f32).astype(jnp.bfloat16)]
    ppermute x6 -> x0, waiting for transfers between devices: 28.5 us -> none  [passed_along(): return lax.ppermute(block, axis, route)]
    reduce_scatter x1 -> x0, waiting for transfers between devices: 17.2 us -> none  [shards(): lax.psum_scatter(jnp.dot(attended, full_out, preferred_element_type=jnp.f...]
    ppermute x6 -> x0, starting transfers between devices: 16.6 us -> none  [passed_along(): return lax.ppermute(block, axis, route)]
  transfers between devices with their start and end apart: 11 -> 2, of which waited for: 7 -> 1; matrix products, arithmetic and copies ran while one was open for 27% -> 2% of each run, Pallas kernels for 0% -> 53%
where the time goes in v1:
time: 209 us; the launch traced here: 208 us
  Pallas kernels  111 us (53%)
  waiting for transfers between devices  71.2 us (34%)
  between operations  14.2 us (7%)
  matrix products  5.94 us (3%)
  local copies, waits for them, and re-layouts  4.36 us (2%)
    pallas_call x1, Pallas kernels, shards(): pl.pallas_call(functools.partial(project_kernel, n, n_tp, group, far), ou...  79.2 us
    all_gather x1, waiting for transfers between devices, shards(): full_out = lax.all_gather(w_out, 'sp', axis=1, tiled=True)  70.5 us
    pallas_call x1, Pallas kernels, shards(): pl.pallas_call(functools.partial(attend_kernel, heads), out_shape=(jax.Sh...  19.1 us
    pallas_call x1, Pallas kernels, shards(): pl.pallas_call(functools.partial(return_kernel, n_tp, group), out_shape=(...  12.9 us
    dot_general x1, matrix products, shards(): jnp.dot(attended, full_out, preferred_element_type=f32).astype(jnp.bfloat16)  5.94 us
  transfers between devices with their start and end apart: 2, of which 1 were waited for; matrix products, arithmetic and copies ran while one was open for 2% of the time, Pallas kernels for 53%

profile of v1, /device:TPU:17, one launch (start us, length us, event | category | flops | bytes accessed | tf_op | source)
XLA Modules:
  0.0 208.3 jit_solution(4437165942698187677)
XLA Ops:
  7.2 0.0 copy-start.2
  7.2 0.0 copy-start.3
  7.2 0.0 copy-start.4
  7.2 0.0 all-gather.3.cloned.1.call-start
  7.2 0.7 all-gather.3.cloned.1.call-update
  7.9 0.0 all-gather.5.cloned.1.call-start
  8.0 70.5 %all-gather.3.cloned.1.call-done = bf16[512,3072]{0,1:T(8,128)(2,1)} async-done(((bf16[512,192]{0,1:T(8,128)(2,1)}), bf16[512,3072]{0,1:T(8,128)(2,1)}) %all-gather.3.cloned.1.call-update) | async-done | bytes 3145744 | tf_op jit(solution)/shard_map/all_gather | solution.py:357
  78.5 0.0 all-gather.5.cloned.1.call-update
  78.5 0.0 copy-done.2
  78.5 0.1 stack.12
  78.6 0.3 copy.10
  78.9 0.0 copy-done.3
  78.9 0.1 stack.13
  79.0 0.3 copy.11
  79.3 0.0 copy-done.4
  79.3 0.1 stack.14
  79.3 0.3 copy.12
  79.6 1.4 maximum_bitcast_fusion
  81.0 0.5 reshape.21.w_ref
  81.6 79.2 %project.1 = (bf16[2048,128]{1,0:T(8,128)(2,1)S(1)}, bf16[2048,256]{1,0:T(8,128)(2,1)S(1)}, bf16[1,2048,256]{2,1,0:T(8,128)(2,1)S(1)}) custom-call(bf16[4,192,384]{2,1,0:T(8,128)(2,1)S(1)} %reshape.21.w_ref, bf16[512,3072]{1,0:T(8,128)(2,1)} %tok_ref.1), custom_call_target="tpu_custom_call" | custom-call | flops 4831838208 | bytes 16777216 | tf_op jit(solution)/shard_map/project/pallas_call | solution.py:365
  160.8 19.1 %attend.1 = (bf16[2048,128]{1,0:T(8,128)(2,1)S(1)}, f32[4,2,512]{2,1,0:T(2,128)S(1)}) custom-call(s32[1]{0:T(128)} %bitcast.base_ref, bf16[2048,128]{1,0:T(8,128)(2,1)S(1)} %get-tuple-element.9.q_ref, bf16[2048,256]{1,0:T(8,128)(2,1)S(1)} %get-tuple-element.10.kv_ref, bf16[1,2048,256]{2,1,0:T(8,128)(2,1)S(1)} %get-tuple-element.11.halo_ref), custom_call_target="tpu_custom_call" | custom-call | flops 4294967296 | bytes 4194304 | tf_op jit(solution)/shard_map/attend/pallas_call | solution.py:393
  179.9 0.0 copy-start
  179.9 0.8 copy-done
  180.7 0.0 copy-start.1
  180.7 0.6 copy-done.1
  181.3 12.9 %hand_back.1 = (bf16[256,1024]{1,0:T(8,128)(2,1)}, f32[4,2,512]{2,1,0:T(2,128)}) custom-call(bf16[2048,128]{1,0:T(8,128)(2,1)} %copy-done, f32[4,2,512]{2,1,0:T(2,128)} %copy-done.1), custom_call_target="tpu_custom_call" | custom-call | tf_op jit(solution)/shard_map/hand_back/pallas_call | solution.py:410
  194.1 1.3 reshape.22
  195.5 0.0 all-gather.5.cloned.1.call-done
  195.5 5.9 %convolution_convert_fusion = bf16[256,3072]{1,0:T(8,128)(2,1)} fusion(bf16[256,1024]{1,0:T(8,128)(2,1)} %get-tuple-element.14, bf16[1024,3072]{0,1:T(8,128)(2,1)} %all-gather.5.cloned.1.call-done), kind=kOutput, calls=%fused_computation | convolution fusion | flops 1611399168 | bytes 8388608 | tf_op jit(solution)/shard_map/dot_general | solution.py:425
Async XLA Ops:
  7.2 71.4 %copy-start.2 = (bf16[192,512]{1,0:T(8,128)(2,1)S(1)}, bf16[192,512]{1,0:T(8,128)(2,1)}, u32[]{:S(2)}) copy-start(bf16[192,512]{1,0:T(8,128)(2,1)} %param.6) | copy-start | bytes 589828
  7.2 71.7 %copy-start.3 = (bf16[192,512]{1,0:T(8,128)(2,1)S(1)}, bf16[192,512]{1,0:T(8,128)(2,1)}, u32[]{:S(2)}) copy-start(bf16[192,512]{1,0:T(8,128)(2,1)} %param.7) | copy-start | bytes 589828
  7.2 72.1 %copy-start.4 = (bf16[192,512]{1,0:T(8,128)(2,1)S(1)}, bf16[192,512]{1,0:T(8,128)(2,1)}, u32[]{:S(2)}) copy-start(bf16[192,512]{1,0:T(8,128)(2,1)} %param.8) | copy-start | bytes 589828
  7.2 71.3 %all-gather.3.cloned.1.call-start = ((), (), s32[]{:S(2)}) async-start(), calls=%async_computation | async-start | bytes 3342336 | tf_op jit(solution)/shard_map/all_gather | solution.py:357
  7.9 187.5 %all-gather.5.cloned.1.call-start = ((), (), s32[]{:S(2)}) async-start(), calls=%async_computation.1 | async-start | bytes 9437184 | tf_op jit(solution)/shard_map/all_gather | solution.py:358
  179.9 0.8 copy-start
  180.7 0.6 copy-start.1
Sparse Core Ops, SparseCore 0:
  10.8 67.6 all-gather.2
  80.0 17.2 all-gather.4

commit v2 on v1

--- a/solution.py
+++ b/solution.py
@@ -208,9 +208,92 @@
             lax.fori_loop(1, planes, lambda k, _, i=i: (w_to_plane(i, k).wait_send(), _)[1], 0)
 
 
-def attend_kernel(heads, base_ref, q_ref, kv_ref, halo_ref, att_ref, lse_ref, qs, ks, vs, top_s, den_s, acc_s):
-    base = base_ref[0]
+def attend_kernel(
+    n, n_tp, group, heads, q_ref, kv_ref, halo_ref, o_ref, mixed_ref, lse_all,
+    qs, ks, vs, top_s, den_s, acc_s, att, lse_ref, o_all, att_all, sums, sums_in,
+    z_send, z_recv, b_send, b_recv, c_send, c_recv, a_send, a_recv, l_send, l_recv, s_send, s_recv, own_sem,
+):
+    sp, tp = lax.axis_index("sp"), lax.axis_index("tp")
+    planes = n // group
+    g, plane = lax.rem(sp, group), sp // group
     own = q_ref.shape[0]
+    base = plane * own
+    rows = lse_all.shape[2]
+    part = mixed_ref.shape[0]
+    cut, width = o_ref.shape
+    half = cut // 2
+
+    def mate(i):
+        return plane * group + (g ^ i)
+
+    barrier = pltpu.get_barrier_semaphore()
+
+    def greet(k, _):
+        pl.semaphore_signal(barrier, inc=1, device_id=at(lax.rem(sp + k * group, n), tp), device_id_type=MESH)
+        return _
+
+    lax.fori_loop(1, planes, greet, 0)
+    for i in range(1, group):
+        pl.semaphore_signal(barrier, inc=1, device_id=at(mate(i), tp), device_id_type=MESH)
+    for j in range(1, n_tp):
+        pl.semaphore_signal(barrier, inc=1, device_id=at(sp, lax.rem(tp + j, n_tp)), device_id_type=MESH)
+
+    def strip(k, i, part_of=None):
+        origin = lax.rem(plane + planes - k, planes) * group + (g ^ i)
+        if part_of is None:
+            return o_all.at[pl.ds(pl.multiple_of(origin * cut, cut), cut)]
+        return o_all.at[pl.ds(pl.multiple_of(origin * cut + part_of * half, half), half)]
+
+    def z_out(k):
+        return pltpu.make_async_remote_copy(
+            src_ref=o_ref, dst_ref=strip(0, 0), send_sem=z_send.at[k], recv_sem=z_recv.at[k],
+            device_id=at(lax.rem(sp + k * group, n), tp), device_id_type=MESH)
+
+    def z_in(k):
+        return pltpu.make_async_remote_copy(
+            src_ref=o_ref, dst_ref=strip(k, 0), send_sem=z_send.at[k], recv_sem=z_recv.at[k],
+            device_id=at(lax.rem(sp + k * group, n), tp), device_id_type=MESH)
+
+    def side_out(k, i):
+        return pltpu.make_async_remote_copy(
+            src_ref=strip(k, 0), dst_ref=strip(k, 0), send_sem=b_send.at[k, i], recv_sem=b_recv.at[k, i],
+            device_id=at(mate(i), tp), device_id_type=MESH)
+
+    def side_in(k, i):
+        return pltpu.make_async_remote_copy(
+            src_ref=strip(k, i), dst_ref=strip(k, i), send_sem=b_send.at[k, i], recv_sem=b_recv.at[k, i],
+            device_id=at(mate(i), tp), device_id_type=MESH)
+
+    def corner_out(k, i):
+        return pltpu.make_async_remote_copy(
+            src_ref=strip(k, i, i - 1), dst_ref=strip(k, i, i - 1), send_sem=c_send.at[k, i], recv_sem=c_recv.at[k, i],
+            device_id=at(mate(3 - i), tp), device_id_type=MESH)
+
+    def corner_in(k, i):
+        return pltpu.make_async_remote_copy(
+            src_ref=strip(k, 3, i - 1), dst_ref=strip(k, 3, i - 1), send_sem=c_send.at[k, i], recv_sem=c_recv.at[k, i],
+            device_id=at(mate(3 - i), tp), device_id_type=MESH)
+
+    near = [i for i in (1, 2) if i < group]
+
+    def sides(k):
+        for i in near:
+            side_out(k, i).start()
+
+    def corners(k):
+        for i in near:
+            side_in(k, i).wait_recv()
+            if group == 4:
+                corner_out(k, i).start()
+
+    own_o = pltpu.make_async_copy(o_ref, strip(0, 0), own_sem.at[0])
+    own_o.start()
+    pl.semaphore_wait(barrier, planes - 1 + group - 1 + n_tp - 1)
+    if planes > 1:
+        lax.fori_loop(1, planes, lambda k, _: (z_out(k).start(), _)[1], 0)
+    own_o.wait()
+    sides(0)
+
     behind = ks.shape[0] - own
     pieces, piece_rows = halo_ref.shape[0], halo_ref.shape[1]
     qs[...] = q_ref[...].astype(jnp.float32) * HEAD_SIZE ** (-0.5)
@@ -220,6 +303,7 @@
     ks[behind:] = kv_ref[:, :LANES].astype(jnp.float32)
     vs[behind:] = kv_ref[:, LANES:].astype(jnp.float32)
 
+    passed = 0
     for number, d in enumerate(dilation_rates):
         step = min(KEYS_BEHIND, own // d)
         count = own // d // step
@@ -264,79 +348,112 @@
             return _
 
         lax.fori_loop(0, d * count, block, 0, unroll=2)
-
-    rows = lse_ref.shape[2]
-    att_ref[...] = (acc_s[...] / den_s[...]).astype(jnp.bfloat16)
+        if number + 1 < len(dilation_rates) and passed + 1 < planes:
+            z_in(passed + 1).wait_recv()
+            sides(passed + 1)
+            corners(passed)
+            passed += 1
+
+    att[...] = (acc_s[...] / den_s[...]).astype(jnp.bfloat16)
+
+    def att_out(i):
+        mine = pl.ds(pl.multiple_of((g ^ i) * rows, rows), rows)
+        return pltpu.make_async_remote_copy(
+            src_ref=att.at[mine], dst_ref=att_all.at[g], send_sem=a_send.at[i], recv_sem=a_recv.at[i],
+            device_id=at(mate(i), tp), device_id_type=MESH)
+
+    def att_in(i):
+        return pltpu.make_async_remote_copy(
+            src_ref=att.at[pl.ds(0, rows)], dst_ref=att_all.at[g ^ i], send_sem=a_send.at[i], recv_sem=a_recv.at[i],
+            device_id=at(mate(i), tp), device_id_type=MESH)
+
+    def lse_out(i):
+        return pltpu.make_async_remote_copy(
+            src_ref=lse_ref.at[g ^ i], dst_ref=lse_all.at[g], send_sem=l_send.at[i], recv_sem=l_recv.at[i],
+            device_id=at(mate(i), tp), device_id_type=MESH)
+
+    def lse_in(i):
+        return pltpu.make_async_remote_copy(
+            src_ref=lse_ref.at[g ^ i], dst_ref=lse_all.at[g ^ i], send_sem=l_send.at[i], recv_sem=l_recv.at[i],
+            device_id=at(mate(i), tp), device_id_type=MESH)
+
+    for i in range(1, group):
+        att_out(i).start()
+    own_a = pltpu.make_async_copy(att.at[pl.ds(pl.multiple_of(g * rows, rows), rows)], att_all.at[g], own_sem.at[1])
+    own_a.start()
+
     for t in range(own // LANES):
         at_rows = pl.ds(t * LANES, LANES)
         lse = (top_s[at_rows, :] + jnp.log(den_s[at_rows, :])).T
         b, off = (t * LANES) // rows, (t * LANES) % rows
         for h in range(heads):
             lse_ref[b, h : h + 1, off : off + LANES] = lse[h * HEAD_SIZE : h * HEAD_SIZE + 1, :]
-
-
-def return_kernel(n_tp, group, att_ref, lse_ref, all_ref, lse_all, a_send, a_recv, l_send, l_recv, own_sem):
-    sp, tp = lax.axis_index("sp"), lax.axis_index("tp")
-    g, plane = lax.rem(sp, group), sp // group
-    part = all_ref.shape[0]
-    width = all_ref.shape[1] // n_tp
-    others = [(i, j) for i in range(group) for j in range(n_tp) if (i, j) != (0, 0)]
-
-    def device(i, j):
-        return plane * group + (g ^ i), lax.rem(tp + j, n_tp)
-
-    barrier = pltpu.get_barrier_semaphore()
-    for i, j in others:
-        pl.semaphore_signal(barrier, inc=1, device_id=at(*device(i, j)), device_id_type=MESH)
-
-    def columns(h, c):
-        return pl.ds(pl.multiple_of(c * width + h * LANES, LANES), LANES)
-
-    def sent_rows(i, j):
-        c = lax.rem(tp + j, n_tp)
-        return pl.ds(pl.multiple_of((g ^ i) * (part * n_tp) + c * part, part), part)
-
-    own = pltpu.make_async_copy(att_ref.at[sent_rows(0, 0)], all_ref.at[:, columns(g, tp)], own_sem.at[0])
-    own_l = pltpu.make_async_copy(lse_ref.at[g], lse_all.at[g], own_sem.at[1])
-    own.start()
+    for i in range(1, group):
+        lse_out(i).start()
+    own_l = pltpu.make_async_copy(lse_ref.at[g], lse_all.at[g], own_sem.at[2])
     own_l.start()
-    pl.semaphore_wait(barrier, len(others))
-
-    def out(i, j):
-        return pltpu.make_async_remote_copy(
-            src_ref=att_ref.at[sent_rows(i, j)], dst_ref=all_ref.at[:, columns(g, tp)],
-            send_sem=a_send.at[i, j], recv_sem=a_recv.at[i, j], device_id=at(*device(i, j)), device_id_type=MESH)
-
-    def arrives(i, j):
-        return pltpu.make_async_remote_copy(
-            src_ref=att_ref.at[sent_rows(i, j)],
-            dst_ref=all_ref.at[:, columns(g ^ i, lax.rem(tp + n_tp - j, n_tp))],
-            send_sem=a_send.at[i, j], recv_sem=a_recv.at[i, j], device_id=at(*device(i, j)), device_id_type=MESH)
-
-    def lse_out(i):
-        return pltpu.make_async_remote_copy(
-            src_ref=lse_ref.at[g ^ i], dst_ref=lse_all.at[g], send_sem=l_send.at[i], recv_sem=l_recv.at[i],
-            device_id=at(*device(i, 0)), device_id_type=MESH)
-
-    def lse_in(i):
-        return pltpu.make_async_remote_copy(
-            src_ref=lse_ref.at[g ^ i], dst_ref=lse_all.at[g ^ i], send_sem=l_send.at[i], recv_sem=l_recv.at[i],
-            device_id=at(*device(i, 0)), device_id_type=MESH)
-
-    for i, j in others:
-        out(i, j).start()
-    for i in range(1, group):
-        lse_out(i).start()
-    own.wait()
+
+    if group == 1:
+        if planes - 1 > passed:
+            lax.fori_loop(passed + 1, planes, lambda k, _: (z_in(k).wait_recv(), _)[1], 0)
+    else:
+        while passed + 1 < planes:
+            z_in(passed + 1).wait_recv()
+            sides(passed + 1)
+            corners(passed)
+            passed += 1
+        corners(passed)
+        if group == 4:
+            for k in range(planes):
+                for i in near:
+                    corner_in(k, i).wait_recv()
+
+    own_a.wait()
+    for i in range(1, group):
+        att_in(i).wait_recv()
+
+    chunks, chunk = sums.shape[1], sums.shape[3]
+
+    def product(c, j):
+        wanted = lax.rem(tp + j, n_tp)
+        here = pl.ds(pl.multiple_of(wanted * part, part), part)
+        a = jnp.concatenate([att_all[b, here, :] for b in range(group)], axis=1)
+        w = o_all[c * chunk : (c + 1) * chunk, :]
+        return lax.dot_general(a, w, (((1,), (1,)), ((), ())), preferred_element_type=jnp.float32)
+
+    def sum_out(c, j):
+        return pltpu.make_async_remote_copy(
+            src_ref=sums.at[j, c], dst_ref=sums_in.at[j, c], send_sem=s_send.at[j, c], recv_sem=s_recv.at[j, c],
+            device_id=at(sp, lax.rem(tp + j, n_tp)), device_id_type=MESH)
+
+    for j in range(1, n_tp):
+        for c in range(chunks):
+            sums[j, c] = product(c, j).astype(jnp.bfloat16)
+            sum_out(c, j).start()
+    for c in range(chunks):
+        total = product(c, 0).astype(jnp.bfloat16).astype(jnp.float32)
+        for j in range(1, n_tp):
+            sum_out(c, j).wait_recv()
+            total += sums_in[j, c].astype(jnp.float32)
+        mixed_ref[:, c * chunk : (c + 1) * chunk] = total.astype(jnp.bfloat16)
+
     own_l.wait()
-    for i, j in others:
-        arrives(i, j).wait_recv()
     for i in range(1, group):
         lse_in(i).wait_recv()
-    for i, j in others:
-        out(i, j).wait_send()
-    for i in range(1, group):
+    for j in range(1, n_tp):
+        for c in range(chunks):
+            sum_out(c, j).wait_send()
+    for i in range(1, group):
+        att_out(i).wait_send()
         lse_out(i).wait_send()
+    if planes > 1:
+        lax.fori_loop(1, planes, lambda k, _: (z_out(k).wait_send(), _)[1], 0)
+    if group > 1:
+        for k in range(planes):
+            for i in near:
+                side_out(k, i).wait_send()
+                if group == 4:
+                    corner_out(k, i).wait_send()
 
 
 def shards(n, n_tp, tokens, w_query, w_key, w_value, w_out):
@@ -353,9 +470,6 @@
     own = group * rows
     part = rows // n_tp
     heads = LANES // HEAD_SIZE
-
-    full_out = lax.all_gather(w_out, "sp", axis=1, tiled=True)
-    full_out = lax.all_gather(full_out, "tp", axis=0, tiled=True)
 
     w = jnp.stack([w_query, w_key, w_value], 1).reshape(depth, 3, group, LANES)
     w = w.transpose(2, 0, 1, 3).reshape(group, depth, 3 * LANES)
@@ -387,43 +501,38 @@
         name="project",
     )(w, tokens)
 
-    base = (lax.axis_index("sp") // group * own).astype(jnp.int32).reshape(1)
     behind = far * own
-    f32 = jnp.float32
-    att, lse = pl.pallas_call(
-        functools.partial(attend_kernel, heads),
-        out_shape=(
-            jax.ShapeDtypeStruct((own, LANES), jnp.bfloat16),
-            jax.ShapeDtypeStruct((group, heads, rows), f32),
-        ),
-        in_specs=[pl.BlockSpec(memory_space=pltpu.SMEM), vmem, vmem, vmem],
+    f32, bf16 = jnp.float32, jnp.bfloat16
+    cut = w_out.shape[1]
+    chunks = 4 if (n * cut) % (4 * LANES) == 0 else 1
+    chunk = n * cut // chunks
+    return_shapes = (
+        jax.ShapeDtypeStruct((part, n * cut), bf16),
+        jax.ShapeDtypeStruct((group, heads, rows), f32),
+    )
+    mixed, lse = pl.pallas_call(
+        functools.partial(attend_kernel, n, n_tp, group, heads),
+        out_shape=return_shapes,
+        in_specs=[vmem] * 4,
         out_specs=(vmem, vmem),
         scratch_shapes=[
             VMEM((own, LANES), f32), VMEM((behind + own, LANES), f32), VMEM((behind + own, LANES), f32),
             VMEM((own, LANES), f32), VMEM((own, LANES), f32), VMEM((own, LANES), f32),
+            VMEM((own, LANES), bf16), VMEM((group, heads, rows), f32),
+            VMEM((n * cut, width), bf16), VMEM((group, rows, LANES), bf16),
+            VMEM((n_tp, chunks, part, chunk), bf16), VMEM((n_tp, chunks, part, chunk), bf16),
+            dma((planes,)), dma((planes,)),
+            dma((planes, group)), dma((planes, group)),
+            dma((planes, group)), dma((planes, group)),
+            dma((group,)), dma((group,)), dma((group,)), dma((group,)),
+            dma((n_tp, chunks)), dma((n_tp, chunks)),
+            dma((3,)),
         ],
-        compiler_params=pltpu.CompilerParams(vmem_limit_bytes=32 << 20),
+        compiler_params=pltpu.CompilerParams(collective_id=1, has_side_effects=True, vmem_limit_bytes=48 << 20),
         cost_estimate=pl.CostEstimate(flops=1 << 32, bytes_accessed=1 << 22, transcendentals=1 << 22),
         name="attend",
-    )(base, q, kv, halo)
-
-    attended, lse_all = pl.pallas_call(
-        functools.partial(return_kernel, n_tp, group),
-        out_shape=(
-            jax.ShapeDtypeStruct((part, n_tp * width), jnp.bfloat16),
-            jax.ShapeDtypeStruct((group, heads, rows), f32),
-        ),
-        in_specs=[vmem, vmem],
-        out_specs=(vmem, vmem),
-        scratch_shapes=[
-            dma((group, n_tp)), dma((group, n_tp)), dma((group,)), dma((group,)), dma((2,)),
-        ],
-        compiler_params=pltpu.CompilerParams(collective_id=1, has_side_effects=True),
-        name="hand_back",
-    )(att, lse)
-
-    mixed = jnp.dot(attended, full_out, preferred_element_type=f32).astype(jnp.bfloat16)
-    return mixed, lse_all.reshape(group * heads, rows)
+    )(q, kv, halo, w_out.T)
+    return mixed, lse.reshape(group * heads, rows)
 
 
 def solution(mesh):

time: 209 us -> 137 us (0.66)
  waiting for transfers between devices: 71.2 us -> 0 us
  Pallas kernels: 111 us -> 129 us
  between operations: 14.2 us -> 0.73 us
  matrix products: 5.94 us -> 0 us
    all_gather x2 -> x0, waiting for transfers between devices: 70.5 us -> none  [the longest x1 70.5 us: shards(): full_out = lax.all_gather(w_out, 'sp', axis=1, tiled=True)]
    pallas_call x2 -> x1, Pallas kernels: 31.9 us -> 46.5 us  [shards(): pl.pallas_call(functools.partial(attend_kernel, n, n_tp, group, heads), o...]
    dot_general x1 -> x0, matrix products: 5.94 us -> none  [shards(): jnp.dot(attended, full_out, preferred_element_type=f32).astype(jnp.bfloat16)]
    pallas_call x1, Pallas kernels: 79.2 us -> 82.4 us  [shards(): pl.pallas_call(functools.partial(project_kernel, n, n_tp, group, far), ou...]
  transfers between devices with their start and end apart: 2 -> 0, of which waited for: 1 -> 0; matrix products, arithmetic and copies ran while one was open for 2% -> 0% of each run, Pallas kernels for 53% -> 0%
where the time goes in v2:
time: 137 us; the launch traced here: 136 us
  Pallas kernels  129 us (94%)
  local copies, waits for them, and re-layouts  5.28 us (4%)
    pallas_call x1, Pallas kernels, shards(): pl.pallas_call(functools.partial(project_kernel, n, n_tp, group, far), ou...  82.4 us
    pallas_call x1, Pallas kernels, shards(): pl.pallas_call(functools.partial(attend_kernel, n, n_tp, group, heads), o...  46.5 us
    another operation x6, local copies, waits for them, and re-layouts, shards(): w = jnp.stack([w_query, w_key, w_value], 1).reshape(depth, 3, group, LANES)  2.96 us

profile of v2, /device:TPU:17, one launch (start us, length us, event | category | flops | bytes accessed | tf_op | source)
XLA Modules:
  0.0 136.3 jit_solution(1141880966172143256)
XLA Ops:
  0.6 0.0 copy-start.1
  0.6 1.0 stack.12
  1.7 0.3 copy.10
  2.0 1.0 stack.13
  3.0 0.3 copy.11
  3.3 0.0 copy-done.1
  3.3 0.1 stack.14
  3.3 0.3 copy.12
  3.6 1.4 maximum_bitcast_fusion
  5.0 0.5 reshape.17.w_ref
  5.6 0.0 copy-start
  5.6 82.4 %project.1 = (bf16[2048,128]{1,0:T(8,128)(2,1)S(1)}, bf16[2048,256]{1,0:T(8,128)(2,1)S(1)}, bf16[1,2048,256]{2,1,0:T(8,128)(2,1)S(1)}) custom-call(bf16[4,192,384]{2,1,0:T(8,128)(2,1)S(1)} %reshape.17.w_ref, bf16[512,3072]{1,0:T(8,128)(2,1)} %tok_ref.1), custom_call_target="tpu_custom_call" | custom-call | flops 4831838208 | bytes 16777216 | tf_op jit(solution)/shard_map/project/pallas_call | solution.py:479
  87.9 0.0 copy-done
  87.9 46.5 %attend.1 = (bf16[256,3072]{1,0:T(8,128)(2,1)S(1)}, f32[4,2,512]{2,1,0:T(2,128)S(1)}) custom-call(bf16[2048,128]{1,0:T(8,128)(2,1)S(1)} %get-tuple-element.7.q_ref, bf16[2048,256]{1,0:T(8,128)(2,1)S(1)} %get-tuple-element.8.kv_ref, bf16[1,2048,256]{2,1,0:T(8,128)(2,1)S(1)} %get-tuple-element.9.halo_ref, bf16[192,512]{1,0:T(8,128)(2,1)S(1)} %bitcast.3), custom_call_target="tpu_custom_call" | custom-call | flops 4294967296 | bytes 4194304 | tf_op jit(solution)/shard_map/attend/pallas_call | solution.py:513
  134.5 0.6 reshape.18
  135.1 1.1 copy.14
Async XLA Ops:
  0.6 2.6 %copy-start.1 = (bf16[192,512]{1,0:T(8,128)(2,1)S(1)}, bf16[192,512]{1,0:T(8,128)(2,1)}, u32[]{:S(2)}) copy-start(bf16[192,512]{1,0:T(8,128)(2,1)} %param.8) | copy-start | bytes 589828
  5.6 82.4 %copy-start = (bf16[512,192]{0,1:T(8,128)(2,1)S(1)}, bf16[512,192]{0,1:T(8,128)(2,1)}, u32[]{:S(2)}) copy-start(bf16[512,192]{0,1:T(8,128)(2,1)} %param.9) | copy-start | bytes 589828

commit v3 on v2

--- a/solution.py
+++ b/solution.py
@@ -23,9 +23,9 @@
 
 
 def project_kernel(
-    n, n_tp, group, far, w_ref, tok_ref, q_ref, kv_ref, halo_ref,
-    tok_all, w_all, w1_send, w1_recv, w2_send, w2_recv,
-    t_send, t_recv, d_send, d_recv, f_send, f_recv, h_send, h_recv, own_sem,
+    n, n_tp, group, far, wq_ref, wk_ref, wv_ref, tok_ref, o_ref, q_ref, kv_ref, halo_ref, o_plane,
+    tok_all, w_all, w_ref, pack_sem, w1_send, w1_recv, up_send, up_recv, down_send, down_recv,
+    t_send, t_recv, d_send, d_recv, f_send, f_recv, h_send, h_recv, o_send, o_recv, own_sem,
 ):
     sp, tp = lax.axis_index("sp"), lax.axis_index("tp")
     planes = n // group
@@ -45,9 +45,19 @@
         pl.semaphore_signal(barrier, inc=1, device_id=at(sp, lax.rem(tp + j, n_tp)), device_id_type=MESH)
 
     own_t = pltpu.make_async_copy(tok_ref, tok_all.at[g], own_sem.at[0])
-    own_w = pltpu.make_async_copy(w_ref.at[g], w_all.at[sp], own_sem.at[1])
+    own_o = pltpu.make_async_copy(o_ref, o_plane.at[g], own_sem.at[1])
+
+    def pack(t, i):
+        source = (wq_ref, wk_ref, wv_ref)[t].at[:, pl.ds(pl.multiple_of((g ^ i) * LANES, LANES), LANES)]
+        lanes = pl.ds(t * LANES, LANES)
+        to = w_all.at[sp, :, lanes] if i == 0 else w_ref.at[i, :, lanes]
+        return pltpu.make_async_copy(source, to, pack_sem.at[t, i])
+
+    for i in list(range(1, group)) + [0]:
+        for t in range(3):
+            pack(t, i).start()
     own_t.start()
-    own_w.start()
+    own_o.start()
     pl.semaphore_wait(barrier, n - 1 + n_tp - 1)
 
     def mate(i):
@@ -55,27 +65,63 @@
 
     def w_in_plane(i):
         return pltpu.make_async_remote_copy(
-            src_ref=w_ref.at[g ^ i], dst_ref=w_all.at[sp], send_sem=w1_send.at[i], recv_sem=w1_recv.at[i],
+            src_ref=w_ref.at[i], dst_ref=w_all.at[sp], send_sem=w1_send.at[i], recv_sem=w1_recv.at[i],
             device_id=at(mate(i), tp), device_id_type=MESH)
 
     def w_in_plane_arrives(i):
         return pltpu.make_async_remote_copy(
-            src_ref=w_ref.at[g ^ i], dst_ref=w_all.at[mate(i)], send_sem=w1_send.at[i], recv_sem=w1_recv.at[i],
-            device_id=at(mate(i), tp), device_id_type=MESH)
-
-    def w_to_plane(i, k):
-        source = w_ref.at[g] if i == 0 else w_all.at[mate(i)]
-        return pltpu.make_async_remote_copy(
-            src_ref=source, dst_ref=w_all.at[mate(i)],
-            send_sem=w2_send.at[i, k], recv_sem=w2_recv.at[i, k],
-            device_id=at(lax.rem(sp + k * group, n), tp), device_id_type=MESH)
-
-    def w_to_plane_arrives(i, k):
-        origin = lax.rem(plane + planes - k, planes) * group + (g ^ i)
-        return pltpu.make_async_remote_copy(
-            src_ref=w_ref.at[g], dst_ref=w_all.at[origin],
-            send_sem=w2_send.at[i, k], recv_sem=w2_recv.at[i, k],
-            device_id=at(lax.rem(sp + k * group, n), tp), device_id_type=MESH)
+            src_ref=w_ref.at[i], dst_ref=w_all.at[mate(i)], send_sem=w1_send.at[i], recv_sem=w1_recv.at[i],
+            device_id=at(mate(i), tp), device_id_type=MESH)
+
+    def slab(p, i):
+        return w_all.at[lax.rem(p + 2 * planes, planes) * group + (g ^ i)]
+
+    def up(i, k, p):
+        return pltpu.make_async_remote_copy(
+            src_ref=slab(p, i), dst_ref=slab(p, i), send_sem=up_send.at[i, k], recv_sem=up_recv.at[i, k],
+            device_id=at(lax.rem(sp + group, n), tp), device_id_type=MESH)
+
+    def down(i, k, p):
+        return pltpu.make_async_remote_copy(
+            src_ref=slab(p, i), dst_ref=slab(p, i), send_sem=down_send.at[i, k], recv_sem=down_recv.at[i, k],
+            device_id=at(lax.rem(sp + n - group, n), tp), device_id_type=MESH)
+
+    def when(condition, action):
+        @pl.when(condition)
+        def _():
+            action()
+
+    first, last = plane == 0, plane == planes - 1
+
+    def relay(k, i):
+        when(~last & (plane - k + 1 >= 0), lambda: up(i, k, plane - k + 1).start())
+        when(~first & (plane + k - 1 < planes), lambda: down(i, k, plane + k - 1).start())
+
+    def relayed(k, i):
+        when(plane - k >= 0, lambda: up(i, k, plane - k).wait_recv())
+        when(plane + k < planes, lambda: down(i, k, plane + k).wait_recv())
+
+    def relay_left(k, i):
+        when(~last & (plane - k + 1 >= 0), lambda: up(i, k, plane - k + 1).wait_send())
+        when(~first & (plane + k - 1 < planes), lambda: down(i, k, plane + k - 1).wait_send())
+
+    def hops(body):
+        def one(k, _):
+            for i in range(group):
+                body(k, i)
+            return _
+
+        return one
+
+    def o_out(i):
+        return pltpu.make_async_remote_copy(
+            src_ref=o_ref, dst_ref=o_plane.at[g], send_sem=o_send.at[i], recv_sem=o_recv.at[i],
+            device_id=at(mate(i), tp), device_id_type=MESH)
+
+    def o_in(i):
+        return pltpu.make_async_remote_copy(
+            src_ref=o_ref, dst_ref=o_plane.at[g ^ i], send_sem=o_send.at[i], recv_sem=o_recv.at[i],
+            device_id=at(mate(i), tp), device_id_type=MESH)
 
     mine = pl.ds(pl.multiple_of(tp * part, part), part)
 
@@ -119,31 +165,38 @@
 
     near = [i for i in (1, 2) if i < group]
     for i in range(1, group):
+        for t in range(3):
+            pack(t, i).wait()
         w_in_plane(i).start()
+    for t in range(3):
+        pack(t, 0).wait()
     if planes > 1:
-        lax.fori_loop(1, planes, lambda k, _: (w_to_plane(0, k).start(), _)[1], 0)
+        relay(1, 0)
     for i in near:
         tokens_out(i).start()
     for i in range(1, group):
         w_in_plane_arrives(i).wait_recv()
         if planes > 1:
-            lax.fori_loop(1, planes, lambda k, _, i=i: (w_to_plane(i, k).start(), _)[1], 0)
+            relay(1, i)
+
+    def pass_on(k, i):
+        relayed(k, i)
+        relay(k + 1, i)
+
+    if planes > 1:
+        lax.fori_loop(1, planes - 1, hops(pass_on), 0)
     for i in near:
         tokens_in(i).wait_recv()
         if group == 4:
             corner_out(i).start()
         for j in range(1, n_tp):
             across(i, j).start()
-
-    own_w.wait()
+    for i in range(1, group):
+        o_out(i).start()
+    if planes > 1:
+        for i in range(group):
+            relayed(planes - 1, i)
     own_t.wait()
-    for i in range(group):
-        if planes > 1:
-            lax.fori_loop(1, planes, lambda k, _, i=i: (w_to_plane_arrives(i, k).wait_recv(), _)[1], 0)
-
-    def halo_block(h, b):
-        view = pl.ds(pl.multiple_of(b * rows, rows), rows)
-        return view
 
     def halo_out(h, i):
         view = pl.ds(pl.multiple_of((g ^ i) * rows, rows), rows)
@@ -204,14 +257,17 @@
         if group == 4:
             corner_out(i).wait_send()
     if planes > 1:
-        for i in range(group):
-            lax.fori_loop(1, planes, lambda k, _, i=i: (w_to_plane(i, k).wait_send(), _)[1], 0)
+        lax.fori_loop(1, planes, hops(relay_left), 0)
+    own_o.wait()
+    for i in range(1, group):
+        o_in(i).wait_recv()
+        o_out(i).wait_send()
 
 
 def attend_kernel(
-    n, n_tp, group, heads, q_ref, kv_ref, halo_ref, o_ref, mixed_ref, lse_all,
+    n, n_tp, group, heads, q_ref, kv_ref, halo_ref, o_ref, o_plane, mixed_ref, lse_all,
     qs, ks, vs, top_s, den_s, acc_s, att, lse_ref, o_all, att_all, sums, sums_in,
-    z_send, z_recv, b_send, b_recv, c_send, c_recv, a_send, a_recv, l_send, l_recv, s_send, s_recv, own_sem,
+    z_send, z_recv, b_send, b_recv, c_send, c_recv, a_send, a_recv, l_send, l_recv, s_send, s_recv, own_sem, o_sem,
 ):
     sp, tp = lax.axis_index("sp"), lax.axis_index("tp")
     planes = n // group
@@ -286,13 +342,14 @@
             if group == 4:
                 corner_out(k, i).start()
 
-    own_o = pltpu.make_async_copy(o_ref, strip(0, 0), own_sem.at[0])
-    own_o.start()
+    def settled(i):
+        return pltpu.make_async_copy(o_plane.at[g ^ i], strip(0, i), o_sem.at[i])
+
+    for i in range(group):
+        settled(i).start()
     pl.semaphore_wait(barrier, planes - 1 + group - 1 + n_tp - 1)
     if planes > 1:
         lax.fori_loop(1, planes, lambda k, _: (z_out(k).start(), _)[1], 0)
-    own_o.wait()
-    sides(0)
 
     behind = ks.shape[0] - own
     pieces, piece_rows = halo_ref.shape[0], halo_ref.shape[1]
@@ -351,7 +408,8 @@
         if number + 1 < len(dilation_rates) and passed + 1 < planes:
             z_in(passed + 1).wait_recv()
             sides(passed + 1)
-            corners(passed)
+            if passed > 0:
+                corners(passed)
             passed += 1
 
     att[...] = (acc_s[...] / den_s[...]).astype(jnp.bfloat16)
@@ -400,14 +458,18 @@
         while passed + 1 < planes:
             z_in(passed + 1).wait_recv()
             sides(passed + 1)
+            if passed > 0:
+                corners(passed)
+            passed += 1
+        if passed > 0:
             corners(passed)
-            passed += 1
-        corners(passed)
         if group == 4:
-            for k in range(planes):
+            for k in range(1, planes):
                 for i in near:
                     corner_in(k, i).wait_recv()
 
+    for i in range(group):
+        settled(i).wait()
     own_a.wait()
     for i in range(1, group):
         att_in(i).wait_recv()
@@ -449,7 +511,7 @@
     if planes > 1:
         lax.fori_loop(1, planes, lambda k, _: (z_out(k).wait_send(), _)[1], 0)
     if group > 1:
-        for k in range(planes):
+        for k in range(1, planes):
             for i in near:
                 side_out(k, i).wait_send()
                 if group == 4:
@@ -471,39 +533,43 @@
     part = rows // n_tp
     heads = LANES // HEAD_SIZE
 
-    w = jnp.stack([w_query, w_key, w_value], 1).reshape(depth, 3, group, LANES)
-    w = w.transpose(2, 0, 1, 3).reshape(group, depth, 3 * LANES)
+    turned = w_out.T
+    cut = w_out.shape[1]
 
     dma = pltpu.SemaphoreType.DMA
     vmem = pl.BlockSpec(memory_space=VMEM)
-    q, kv, halo = pl.pallas_call(
+    q, kv, halo, o_plane = pl.pallas_call(
         functools.partial(project_kernel, n, n_tp, group, far),
         out_shape=(
             jax.ShapeDtypeStruct((own, LANES), jnp.bfloat16),
             jax.ShapeDtypeStruct((own, 2 * LANES), jnp.bfloat16),
             jax.ShapeDtypeStruct((far, own, 2 * LANES), jnp.bfloat16),
+            jax.ShapeDtypeStruct((group, cut, width), jnp.bfloat16),
         ),
-        in_specs=[vmem, pl.BlockSpec(memory_space=pl.ANY)],
-        out_specs=(vmem, vmem, vmem),
+        in_specs=[pl.BlockSpec(memory_space=pl.ANY)] * 4 + [vmem],
+        out_specs=(vmem,) * 4,
         scratch_shapes=[
             VMEM((group, rows, model), jnp.bfloat16),
             VMEM((n, depth, 3 * LANES), jnp.bfloat16),
+            VMEM((group, depth, 3 * LANES), jnp.bfloat16),
+            dma((3, group)),
             dma((group,)), dma((group,)),
+            dma((group, planes)), dma((group, planes)),
             dma((group, planes)), dma((group, planes)),
             dma((group,)), dma((group,)),
             dma((group,)), dma((group,)),
             dma((group, n_tp)), dma((group, n_tp)),
             dma((far + 1, group)), dma((far + 1, group)),
+            dma((group,)), dma((group,)),
             dma((2,)),
         ],
         compiler_params=pltpu.CompilerParams(collective_id=0, has_side_effects=True, vmem_limit_bytes=48 << 20),
         cost_estimate=pl.CostEstimate(flops=2 * own * model * 3 * LANES, bytes_accessed=1 << 24, transcendentals=0),
         name="project",
-    )(w, tokens)
+    )(w_query, w_key, w_value, tokens, turned)
 
     behind = far * own
     f32, bf16 = jnp.float32, jnp.bfloat16
-    cut = w_out.shape[1]
     chunks = 4 if (n * cut) % (4 * LANES) == 0 else 1
     chunk = n * cut // chunks
     return_shapes = (
@@ -513,7 +579,7 @@
     mixed, lse = pl.pallas_call(
         functools.partial(attend_kernel, n, n_tp, group, heads),
         out_shape=return_shapes,
-        in_specs=[vmem] * 4,
+        in_specs=[vmem] * 5,
         out_specs=(vmem, vmem),
         scratch_shapes=[
             VMEM((own, LANES), f32), VMEM((behind + own, LANES), f32), VMEM((behind + own, LANES), f32),
@@ -526,12 +592,12 @@
             dma((planes, group)), dma((planes, group)),
             dma((group,)), dma((group,)), dma((group,)), dma((group,)),
             dma((n_tp, chunks)), dma((n_tp, chunks)),
-            dma((3,)),
+            dma((3,)), dma((group,)),
         ],
         compiler_params=pltpu.CompilerParams(collective_id=1, has_side_effects=True, vmem_limit_bytes=48 << 20),
         cost_estimate=pl.CostEstimate(flops=1 << 32, bytes_accessed=1 << 22, transcendentals=1 << 22),
         name="attend",
-    )(q, kv, halo, w_out.T)
+    )(q, kv, halo, turned, o_plane)
     return mixed, lse.reshape(group * heads, rows)
 
 

time: 137 us -> 133 us (0.971)
  Pallas kernels: 129 us -> 127 us
    pallas_call x1, Pallas kernels: 82.4 us -> 76.2 us  [shards(): pl.pallas_call(functools.partial(project_kernel, n, n_tp, group, far), ou...]
    pallas_call x1, Pallas kernels: 46.5 us -> 50.5 us  [shards(): pl.pallas_call(functools.partial(attend_kernel, n, n_tp, group, heads), o...]
    unnamed x5 -> x11, local copies, waits for them, and re-layouts: 1.15 us -> 4.84 us
    another operation x6 -> x0, local copies, waits for them, and re-layouts: 2.96 us -> none  [shards(): w = jnp.stack([w_query, w_key, w_value], 1).reshape(depth, 3, group, LANES)]
where the time goes in v3:
time: 133 us
  Pallas kernels  127 us (95%)
  local copies, waits for them, and re-layouts  5.46 us (4%)
    pallas_call x1, Pallas kernels, shards(): pl.pallas_call(functools.partial(project_kernel, n, n_tp, group, far), ou...  76.2 us
    pallas_call x1, Pallas kernels, shards(): pl.pallas_call(functools.partial(attend_kernel, n, n_tp, group, heads), o...  50.5 us
    unnamed x11, local copies, waits for them, and re-layouts  4.84 us

profile of v3, /device:TPU:17, one launch (start us, length us, event | category | flops | bytes accessed | tf_op | source)
XLA Modules:
  0.0 132.9 jit_solution(10690414479746015854)
XLA Ops:
  0.6 0.0 copy-start
  0.6 0.9 copy-done
  1.6 0.0 copy-start.1
  1.6 0.9 copy-done.1
  2.5 0.0 copy-start.2
  2.5 0.9 copy-done.2
  3.4 0.0 copy-start.3
  3.4 0.9 copy-done.3
  4.3 0.0 copy-start.4
  4.3 76.2 %project.1 = (bf16[2048,128]{1,0:T(8,128)(2,1)S(1)}, bf16[2048,256]{1,0:T(8,128)(2,1)S(1)}, bf16[1,2048,256]{2,1,0:T(8,128)(2,1)S(1)}, bf16[4,192,512]{2,1,0:T(8,128)(2,1)S(1)}) custom-call(bf16[192,512]{1,0:T(8,128)(2,1)S(1)} %copy-done, bf16[192,512]{1,0:T(8,128)(2,1)S(1)} %copy-done.1, bf16[192,512]{1,0:T(8,128)(2,1)S(1)} %copy-done.2, ...), custom_call_target="tpu_custom_call" | custom-call | flops 4831838208 | bytes 16777216 | tf_op jit(solution)/shard_map/project/pallas_call | solution.py:541
  80.6 0.0 copy-done.4
  80.6 50.5 %attend.1 = (bf16[256,3072]{1,0:T(8,128)(2,1)S(1)}, f32[4,2,512]{2,1,0:T(2,128)S(1)}) custom-call(bf16[2048,128]{1,0:T(8,128)(2,1)S(1)} %get-tuple-element.8.q_ref, bf16[2048,256]{1,0:T(8,128)(2,1)S(1)} %get-tuple-element.9.kv_ref, bf16[1,2048,256]{2,1,0:T(8,128)(2,1)S(1)} %get-tuple-element.10.halo_ref, bf16[192,512]{1,0:T(8,128)(2,1)S(1)} %bitcast.2, ...), custom_call_target="tpu_custom_call" | custom-call | flops 4294967296 | bytes 4194304 | tf_op jit(solution)/shard_map/attend/pallas_call | solution.py:579
  131.1 0.6 reshape.7
  131.7 1.1 copy.8
Async XLA Ops:
  0.6 0.9 copy-start
  1.6 0.9 copy-start.1
  2.5 0.9 copy-start.2
  3.4 0.9 copy-start.3
  4.3 76.2 %copy-start.4 = (bf16[512,192]{0,1:T(8,128)(2,1)S(1)}, bf16[512,192]{0,1:T(8,128)(2,1)}, u32[]{:S(2)}) copy-start(bf16[512,192]{0,1:T(8,128)(2,1)} %param.9) | copy-start | bytes 589828

commit v4 on v3

--- a/solution.py
+++ b/solution.py
@@ -461,13 +461,6 @@
             if passed > 0:
                 corners(passed)
             passed += 1
-        if passed > 0:
-            corners(passed)
-        if group == 4:
-            for k in range(1, planes):
-                for i in near:
-                    corner_in(k, i).wait_recv()
-
     for i in range(group):
         settled(i).wait()
     own_a.wait()
@@ -475,12 +468,19 @@
         att_in(i).wait_recv()
 
     chunks, chunk = sums.shape[1], sums.shape[3]
+    by_plane = group > 1
+
+    def columns_of(k):
+        if by_plane:
+            c = lax.rem(plane + planes - k, planes)
+            return pl.ds(pl.multiple_of(c * chunk, chunk), chunk)
+        return pl.ds(k * chunk, chunk)
 
     def product(c, j):
         wanted = lax.rem(tp + j, n_tp)
         here = pl.ds(pl.multiple_of(wanted * part, part), part)
         a = jnp.concatenate([att_all[b, here, :] for b in range(group)], axis=1)
-        w = o_all[c * chunk : (c + 1) * chunk, :]
+        w = o_all[columns_of(c), :]
         return lax.dot_general(a, w, (((1,), (1,)), ((), ())), preferred_element_type=jnp.float32)
 
     def sum_out(c, j):
@@ -488,16 +488,30 @@
             src_ref=sums.at[j, c], dst_ref=sums_in.at[j, c], send_sem=s_send.at[j, c], recv_sem=s_recv.at[j, c],
             device_id=at(sp, lax.rem(tp + j, n_tp)), device_id_type=MESH)
 
-    for j in range(1, n_tp):
-        for c in range(chunks):
+    def for_others(c):
+        for j in range(1, n_tp):
             sums[j, c] = product(c, j).astype(jnp.bfloat16)
             sum_out(c, j).start()
-    for c in range(chunks):
+
+    def for_self(c):
         total = product(c, 0).astype(jnp.bfloat16).astype(jnp.float32)
         for j in range(1, n_tp):
             sum_out(c, j).wait_recv()
             total += sums_in[j, c].astype(jnp.float32)
-        mixed_ref[:, c * chunk : (c + 1) * chunk] = total.astype(jnp.bfloat16)
+        mixed_ref[:, columns_of(c)] = total.astype(jnp.bfloat16)
+
+    for c in range(chunks):
+        if group == 4 and c > 0:
+            for i in near:
+                corner_in(c, i).wait_recv()
+        for_others(c)
+        if by_plane and c == 0 and passed > 0:
+            corners(passed)
+        if 0 < c < chunks - 1:
+            for_self(c - 1)
+    if chunks > 1:
+        for_self(chunks - 2)
+    for_self(chunks - 1)
 
     own_l.wait()
     for i in range(1, group):
@@ -546,7 +560,7 @@
             jax.ShapeDtypeStruct((far, own, 2 * LANES), jnp.bfloat16),
             jax.ShapeDtypeStruct((group, cut, width), jnp.bfloat16),
         ),
-        in_specs=[pl.BlockSpec(memory_space=pl.ANY)] * 4 + [vmem],
+        in_specs=[pl.BlockSpec(memory_space=pltpu.HBM)] * 4 + [vmem],
         out_specs=(vmem,) * 4,
         scratch_shapes=[
             VMEM((group, rows, model), jnp.bfloat16),
@@ -570,7 +584,7 @@
 
     behind = far * own
     f32, bf16 = jnp.float32, jnp.bfloat16
-    chunks = 4 if (n * cut) % (4 * LANES) == 0 else 1
+    chunks = planes if group > 1 else (4 if (n * cut) % (4 * LANES) == 0 else 1)
     chunk = n * cut // chunks
     return_shapes = (
         jax.ShapeDtypeStruct((part, n * cut), bf16),

time: 133 us -> 131 us (0.985)
  Pallas kernels: 127 us -> 125 us
    pallas_call x1, Pallas kernels: 50.5 us -> 48.5 us  [shards(): pl.pallas_call(functools.partial(attend_kernel, n, n_tp, group, heads), o...]
where the time goes in v4:
time: 131 us
  Pallas kernels  125 us (95%)
  local copies, waits for them, and re-layouts  5.46 us (4%)
    pallas_call x1, Pallas kernels, shards(): pl.pallas_call(functools.partial(project_kernel, n, n_tp, group, far), ou...  76.2 us
    pallas_call x1, Pallas kernels, shards(): pl.pallas_call(functools.partial(attend_kernel, n, n_tp, group, heads), o...  48.5 us
    unnamed x11, local copies, waits for them, and re-layouts  4.84 us

profile of v4, /device:TPU:17, one launch (start us, length us, event | category | flops | bytes accessed | tf_op | source)
XLA Modules:
  0.0 130.9 jit_solution(4753740449739526540)
XLA Ops:
  0.6 0.0 copy-start
  0.6 0.9 copy-done
  1.6 0.0 copy-start.1
  1.6 0.9 copy-done.1
  2.5 0.0 copy-start.2
  2.5 0.9 copy-done.2
  3.4 0.0 copy-start.3
  3.4 0.9 copy-done.3
  4.3 0.0 copy-start.4
  4.3 76.2 %project.1 = (bf16[2048,128]{1,0:T(8,128)(2,1)S(1)}, bf16[2048,256]{1,0:T(8,128)(2,1)S(1)}, bf16[1,2048,256]{2,1,0:T(8,128)(2,1)S(1)}, bf16[4,192,512]{2,1,0:T(8,128)(2,1)S(1)}) custom-call(bf16[192,512]{1,0:T(8,128)(2,1)S(1)} %copy-done, bf16[192,512]{1,0:T(8,128)(2,1)S(1)} %copy-done.1, bf16[192,512]{1,0:T(8,128)(2,1)S(1)} %copy-done.2, ...), custom_call_target="tpu_custom_call" | custom-call | flops 4831838208 | bytes 16777216 | tf_op jit(solution)/shard_map/project/pallas_call | solution.py:555
  80.6 0.0 copy-done.4
  80.6 48.5 %attend.1 = (bf16[256,3072]{1,0:T(8,128)(2,1)S(1)}, f32[4,2,512]{2,1,0:T(2,128)S(1)}) custom-call(bf16[2048,128]{1,0:T(8,128)(2,1)S(1)} %get-tuple-element.8.q_ref, bf16[2048,256]{1,0:T(8,128)(2,1)S(1)} %get-tuple-element.9.kv_ref, bf16[1,2048,256]{2,1,0:T(8,128)(2,1)S(1)} %get-tuple-element.10.halo_ref, bf16[192,512]{1,0:T(8,128)(2,1)S(1)} %bitcast.2, ...), custom_call_target="tpu_custom_call" | custom-call | flops 4294967296 | bytes 4194304 | tf_op jit(solution)/shard_map/attend/pallas_call | solution.py:593
  129.1 0.6 reshape.7
  129.7 1.1 copy.8
Async XLA Ops:
  0.6 0.9 copy-start
  1.6 0.9 copy-start.1
  2.5 0.9 copy-start.2
  3.4 0.9 copy-start.3
  4.3 76.2 %copy-start.4 = (bf16[512,192]{0,1:T(8,128)(2,1)S(1)}, bf16[512,192]{0,1:T(8,128)(2,1)}, u32[]{:S(2)}) copy-start(bf16[512,192]{0,1:T(8,128)(2,1)} %param.9) | copy-start | bytes 589828

commit v5 on v4

--- a/solution.py
+++ b/solution.py
@@ -23,9 +23,9 @@
 
 
 def project_kernel(
-    n, n_tp, group, far, wq_ref, wk_ref, wv_ref, tok_ref, o_ref, q_ref, kv_ref, halo_ref, o_plane,
+    n, n_tp, group, far, wq_ref, wk_ref, wv_ref, tok_ref, o_ref, q_ref, kv_ref, halo_ref, o_plane, o_far,
     tok_all, w_all, w_ref, pack_sem, w1_send, w1_recv, up_send, up_recv, down_send, down_recv,
-    t_send, t_recv, d_send, d_recv, f_send, f_recv, h_send, h_recv, o_send, o_recv, own_sem,
+    t_send, t_recv, d_send, d_recv, f_send, f_recv, h_send, h_recv, o_send, o_recv, z_send, z_recv, own_sem,
 ):
     sp, tp = lax.axis_index("sp"), lax.axis_index("tp")
     planes = n // group
@@ -164,6 +164,11 @@
             device_id=at(sp, lax.rem(tp + j, n_tp)), device_id_type=MESH)
 
     near = [i for i in (1, 2) if i < group]
+    def z_out(k):
+        return pltpu.make_async_remote_copy(
+            src_ref=o_ref, dst_ref=o_far.at[k], send_sem=z_send.at[k], recv_sem=z_recv.at[k],
+            device_id=at(lax.rem(sp + k * group, n), tp), device_id_type=MESH)
+
     for i in range(1, group):
         for t in range(3):
             pack(t, i).wait()
@@ -184,6 +189,7 @@
         relay(k + 1, i)
 
     if planes > 1:
+        lax.fori_loop(1, planes, lambda k, _: (z_out(k).start(), _)[1], 0)
         lax.fori_loop(1, planes - 1, hops(pass_on), 0)
     for i in near:
         tokens_in(i).wait_recv()
@@ -258,6 +264,7 @@
             corner_out(i).wait_send()
     if planes > 1:
         lax.fori_loop(1, planes, hops(relay_left), 0)
+        lax.fori_loop(1, planes, lambda k, _: (z_out(k).wait(), _)[1], 0)
     own_o.wait()
     for i in range(1, group):
         o_in(i).wait_recv()
@@ -265,9 +272,9 @@
 
 
 def attend_kernel(
-    n, n_tp, group, heads, q_ref, kv_ref, halo_ref, o_ref, o_plane, mixed_ref, lse_all,
+    n, n_tp, group, heads, q_ref, kv_ref, halo_ref, o_far, o_plane, mixed_ref, lse_all,
     qs, ks, vs, top_s, den_s, acc_s, att, lse_ref, o_all, att_all, sums, sums_in,
-    z_send, z_recv, b_send, b_recv, c_send, c_recv, a_send, a_recv, l_send, l_recv, s_send, s_recv, own_sem, o_sem,
+    z_recv, b_send, b_recv, c_send, c_recv, a_send, a_recv, l_send, l_recv, s_send, s_recv, own_sem, o_sem,
 ):
     sp, tp = lax.axis_index("sp"), lax.axis_index("tp")
     planes = n // group
@@ -276,7 +283,7 @@
     base = plane * own
     rows = lse_all.shape[2]
     part = mixed_ref.shape[0]
-    cut, width = o_ref.shape
+    cut, width = o_plane.shape[1:]
     half = cut // 2
 
     def mate(i):
@@ -284,11 +291,6 @@
 
     barrier = pltpu.get_barrier_semaphore()
 
-    def greet(k, _):
-        pl.semaphore_signal(barrier, inc=1, device_id=at(lax.rem(sp + k * group, n), tp), device_id_type=MESH)
-        return _
-
-    lax.fori_loop(1, planes, greet, 0)
     for i in range(1, group):
         pl.semaphore_signal(barrier, inc=1, device_id=at(mate(i), tp), device_id_type=MESH)
     for j in range(1, n_tp):
@@ -300,19 +302,12 @@
             return o_all.at[pl.ds(pl.multiple_of(origin * cut, cut), cut)]
         return o_all.at[pl.ds(pl.multiple_of(origin * cut + part_of * half, half), half)]
 
-    def z_out(k):
-        return pltpu.make_async_remote_copy(
-            src_ref=o_ref, dst_ref=strip(0, 0), send_sem=z_send.at[k], recv_sem=z_recv.at[k],
-            device_id=at(lax.rem(sp + k * group, n), tp), device_id_type=MESH)
-
     def z_in(k):
-        return pltpu.make_async_remote_copy(
-            src_ref=o_ref, dst_ref=strip(k, 0), send_sem=z_send.at[k], recv_sem=z_recv.at[k],
-            device_id=at(lax.rem(sp + k * group, n), tp), device_id_type=MESH)
+        return pltpu.make_async_copy(o_far.at[k], strip(k, 0), z_recv.at[k])
 
     def side_out(k, i):
         return pltpu.make_async_remote_copy(
-            src_ref=strip(k, 0), dst_ref=strip(k, 0), send_sem=b_send.at[k, i], recv_sem=b_recv.at[k, i],
+            src_ref=o_far.at[k], dst_ref=strip(k, 0), send_sem=b_send.at[k, i], recv_sem=b_recv.at[k, i],
             device_id=at(mate(i), tp), device_id_type=MESH)
 
     def side_in(k, i):
@@ -347,9 +342,12 @@
 
     for i in range(group):
         settled(i).start()
-    pl.semaphore_wait(barrier, planes - 1 + group - 1 + n_tp - 1)
     if planes > 1:
-        lax.fori_loop(1, planes, lambda k, _: (z_out(k).start(), _)[1], 0)
+        lax.fori_loop(1, planes, lambda k, _: (z_in(k).start(), _)[1], 0)
+    pl.semaphore_wait(barrier, group - 1 + n_tp - 1)
+    if group > 1:
+        for k in range(1, planes):
+            sides(k)
 
     behind = ks.shape[0] - own
     pieces, piece_rows = halo_ref.shape[0], halo_ref.shape[1]
@@ -406,11 +404,8 @@
 
         lax.fori_loop(0, d * count, block, 0, unroll=2)
         if number + 1 < len(dilation_rates) and passed + 1 < planes:
-            z_in(passed + 1).wait_recv()
-            sides(passed + 1)
-            if passed > 0:
-                corners(passed)
             passed += 1
+            corners(passed)
 
     att[...] = (acc_s[...] / den_s[...]).astype(jnp.bfloat16)
 
@@ -451,16 +446,11 @@
     own_l = pltpu.make_async_copy(lse_ref.at[g], lse_all.at[g], own_sem.at[2])
     own_l.start()
 
-    if group == 1:
-        if planes - 1 > passed:
-            lax.fori_loop(passed + 1, planes, lambda k, _: (z_in(k).wait_recv(), _)[1], 0)
-    else:
-        while passed + 1 < planes:
-            z_in(passed + 1).wait_recv()
-            sides(passed + 1)
-            if passed > 0:
-                corners(passed)
-            passed += 1
+    while group > 1 and passed + 1 < planes:
+        passed += 1
+        corners(passed)
+    if planes > 1:
+        lax.fori_loop(1, planes, lambda k, _: (z_in(k).wait(), _)[1], 0)
     for i in range(group):
         settled(i).wait()
     own_a.wait()
@@ -505,8 +495,6 @@
             for i in near:
                 corner_in(c, i).wait_recv()
         for_others(c)
-        if by_plane and c == 0 and passed > 0:
-            corners(passed)
         if 0 < c < chunks - 1:
             for_self(c - 1)
     if chunks > 1:
@@ -522,8 +510,6 @@
     for i in range(1, group):
         att_out(i).wait_send()
         lse_out(i).wait_send()
-    if planes > 1:
-        lax.fori_loop(1, planes, lambda k, _: (z_out(k).wait_send(), _)[1], 0)
     if group > 1:
         for k in range(1, planes):
             for i in near:
@@ -552,16 +538,17 @@
 
     dma = pltpu.SemaphoreType.DMA
     vmem = pl.BlockSpec(memory_space=VMEM)
-    q, kv, halo, o_plane = pl.pallas_call(
+    q, kv, halo, o_plane, o_far = pl.pallas_call(
         functools.partial(project_kernel, n, n_tp, group, far),
         out_shape=(
             jax.ShapeDtypeStruct((own, LANES), jnp.bfloat16),
             jax.ShapeDtypeStruct((own, 2 * LANES), jnp.bfloat16),
             jax.ShapeDtypeStruct((far, own, 2 * LANES), jnp.bfloat16),
             jax.ShapeDtypeStruct((group, cut, width), jnp.bfloat16),
+            jax.ShapeDtypeStruct((planes, cut, width), jnp.bfloat16),
         ),
         in_specs=[pl.BlockSpec(memory_space=pltpu.HBM)] * 4 + [vmem],
-        out_specs=(vmem,) * 4,
+        out_specs=(vmem,) * 5,
         scratch_shapes=[
             VMEM((group, rows, model), jnp.bfloat16),
             VMEM((n, depth, 3 * LANES), jnp.bfloat16),
@@ -574,7 +561,7 @@
             dma((group,)), dma((group,)),
             dma((group, n_tp)), dma((group, n_tp)),
             dma((far + 1, group)), dma((far + 1, group)),
-            dma((group,)), dma((group,)),
+            dma((group,)), dma((group,)), dma((planes,)), dma((planes,)),
             dma((2,)),
         ],
         compiler_params=pltpu.CompilerParams(collective_id=0, has_side_effects=True, vmem_limit_bytes=48 << 20),
@@ -601,7 +588,7 @@
             VMEM((own, LANES), bf16), VMEM((group, heads, rows), f32),
             VMEM((n * cut, width), bf16), VMEM((group, rows, LANES), bf16),
             VMEM((n_tp, chunks, part, chunk), bf16), VMEM((n_tp, chunks, part, chunk), bf16),
-            dma((planes,)), dma((planes,)),
+            dma((planes,)),
             dma((planes, group)), dma((planes, group)),
             dma((planes, group)), dma((planes, group)),
             dma((group,)), dma((group,)), dma((group,)), dma((group,)),
@@ -611,7 +598,7 @@
         compiler_params=pltpu.CompilerParams(collective_id=1, has_side_effects=True, vmem_limit_bytes=48 << 20),
         cost_estimate=pl.CostEstimate(flops=1 << 32, bytes_accessed=1 << 22, transcendentals=1 << 22),
         name="attend",
-    )(q, kv, halo, turned, o_plane)
+    )(q, kv, halo, o_far, o_plane)
     return mixed, lse.reshape(group * heads, rows)
 
 

time: 131 us -> 124 us (0.947)
  the two profiles are of different devices: /device:TPU:17 before, /device:TPU:0 now
where the time goes in v5:
time: 124 us
  Pallas kernels  118 us (95%)
  local copies, waits for them, and re-layouts  5.46 us (4%)
    pallas_call x1, Pallas kernels, shards(): pl.pallas_call(functools.partial(project_kernel, n, n_tp, group, far), ou...  82.4 us
    pallas_call x1, Pallas kernels, shards(): pl.pallas_call(functools.partial(attend_kernel, n, n_tp, group, heads), o...  35.2 us
    unnamed x9, local copies, waits for them, and re-layouts  4.84 us

profile of v5, /device:TPU:0, one launch (start us, length us, event | category | flops | bytes accessed | tf_op | source)
XLA Modules:
  0.0 123.8 jit_solution(18357020382565554043)
XLA Ops:
  0.6 0.0 copy-start
  0.6 0.9 copy-done
  1.6 0.0 copy-start.1
  1.6 0.9 copy-done.1
  2.5 0.0 copy-start.2
  2.5 0.9 copy-done.2
  3.4 0.0 copy-start.3
  3.4 0.9 copy-done.3
  4.3 82.4 %project.1 = (bf16[2048,128]{1,0:T(8,128)(2,1)S(1)}, bf16[2048,256]{1,0:T(8,128)(2,1)S(1)}, bf16[1,2048,256]{2,1,0:T(8,128)(2,1)S(1)}, bf16[4,192,512]{2,1,0:T(8,128)(2,1)S(1)}, bf16[4,192,512]{2,1,0:T(8,128)(2,1)S(1)}) custom-call(bf16[192,512]{1,0:T(8,128)(2,1)S(1)} %copy-done, bf16[192,512]{1,0:T(8,128)(2,1)S(1)} %copy-done.1, ...), custom_call_target="tpu_custom_call" | custom-call | flops 4831838208 | bytes 16777216 | tf_op jit(solution)/shard_map/project/pallas_call | solution.py:541
  86.8 35.2 %attend.1 = (bf16[256,3072]{1,0:T(8,128)(2,1)S(1)}, f32[4,2,512]{2,1,0:T(2,128)S(1)}) custom-call(bf16[2048,128]{1,0:T(8,128)(2,1)S(1)} %get-tuple-element.9.q_ref, bf16[2048,256]{1,0:T(8,128)(2,1)S(1)} %get-tuple-element.10.kv_ref, bf16[1,2048,256]{2,1,0:T(8,128)(2,1)S(1)} %get-tuple-element.11.halo_ref, bf16[4,192,512]{2,1,0:T(8,128)(2,1)S(1)} %get-tuple-element.12.o_far, ...), custom_call_target="tpu_custom_call" | custom-call | flops 4294967296 | bytes 4194304 | tf_op jit(solution)/shard_map/attend/pallas_call | solution.py:580
  122.0 0.6 reshape.7
  122.6 1.1 copy.8
Async XLA Ops:
  0.6 0.9 copy-start
  1.6 0.9 copy-start.1
  2.5 0.9 copy-start.2
  3.4 0.9 copy-start.3
